TPU v7x, 128 devices: a whole 4x4x4 slice. The times are simulated.
128 devices in a mesh: fs: 32 (over z, y, core), tp: 4 (over x).
Axes of the slice: x: 4, y: 4, z: 4, core: 2. Of those that a mesh axis runs over, the one named last changes fastest.
Arguments:
- x_saved: bfloat16 [65536, 2048], P('fs'), may hold values from -6 to 6
- h_saved: bfloat16 [65536, 1024], P('fs', 'tp'), may hold values from -6 to 6
- key_cot: bfloat16 [65536, 1024], P('fs', 'tp'), may hold values from -6 to 6
- value_cot: bfloat16 [65536, 1024], P('fs', 'tp'), may hold values from -6 to 6
- out_cot: bfloat16 [65536, 2048], P('fs'), may hold values from -6 to 6
- w_key: float32 [2048, 1024], P('fs', 'tp'), may hold values from -0.125 to 0.125
- w_value: float32 [2048, 1024], P('fs', 'tp'), may hold values from -0.125 to 0.125
- w_out: float32 [1024, 2048], P('tp', 'fs'), may hold values from -0.1875 to 0.1875
- p_key: bfloat16 [2048, 256], P('fs'), may hold values from -1 to 1, as said below
- p_value: bfloat16 [2048, 256], P('fs'), may hold values from -1 to 1, as said below
- p_out: bfloat16 [2048, 256], P('fs'), may hold values from -1 to 1, as said below
- m_key: float32 [2, 256, 1024], P(None, 'fs', 'tp'), may hold values from -1.5 to 1.5, as said below
- m_value: float32 [2, 256, 1024], P(None, 'fs', 'tp'), may hold values from -1.5 to 1.5, as said below
- m_out: float32 [2, 256, 1024], P(None, 'fs', 'tp'), may hold values from -1.5 to 1.5, as said below
Outputs:
- step_key: float32 [2048, 1024], P('fs', 'tp')
- step_value: float32 [2048, 1024], P('fs', 'tp')
- step_out: float32 [1024, 2048], P('tp', 'fs')
- copy_key: bfloat16 [2048, 1024], P(None, 'tp')
- copy_value: bfloat16 [2048, 1024], P(None, 'tp')
- copy_out: bfloat16 [1024, 2048], P('tp')
- new_m_key: float32 [2, 256, 1024], P(None, 'fs', 'tp')
- new_m_value: float32 [2, 256, 1024], P(None, 'fs', 'tp')
- new_m_out: float32 [2, 256, 1024], P(None, 'fs', 'tp')
Inputs may be any that keep to these rules, and one draw needn't show every extreme that they name: `p_key`: factor entries are real-valued, dense and of full rank. `p_value`: factor entries are real-valued, dense and of full rank. `p_out`: factor entries are real-valued, dense and of full rank. `m_key`: plane 1 (second moments) lies in 0.05 to 1. `m_value`: plane 1 (second moments) lies in 0.05 to 1. `m_out`: plane 1 (second moments) lies in 0.05 to 1.
All inputs are finite; a program needn't handle non-finite values.
Results may differ from a plain program's by a relative error of at most 0.0085.
Values may be sent and summed in bfloat16 or wider, within the bound.
No kernel may reach another device: no remote copies, remote signals or barrier semaphores. Data moves between devices by JAX's collectives and lax.ppermute only.
A program may use at most 128 MiB of HBM per device.

v0:
```python
import jax
import jax.numpy as jnp
from jax import lax
from jax.experimental import pallas as pl
from jax.experimental.pallas import tpu as pltpu
from jax.sharding import Mesh
from jax.sharding import PartitionSpec as P

FS = ("fs_0", "fs_1", "fs_2")
FAR = ("fs_0", "fs_1")
CORE = "fs_2"
MIB = 1024 * 1024

beta_one = 0.9
beta_two = 0.9
learn_rate = 0.01


def vmem():
    return pl.BlockSpec(memory_space=pltpu.VMEM)


def smem():
    return pl.BlockSpec(memory_space=pltpu.SMEM)


def shift(value, axis, by):
    size = lax.axis_size(axis)
    return lax.ppermute(value, axis, [(i, (i + by) % size) for i in range(size)])


def crossed(value, stage, by):
    pairs = []
    for z in range(4):
        for y in range(4):
            for core in range(2):
                if stage == core:
                    target = (z, (y + by) % 4)
                else:
                    target = ((z + by) % 4, y)
                pairs.append(((z * 4 + y) * 2 + core, (target[0] * 4 + target[1]) * 2 + core))
    return lax.ppermute(value, FS, pairs)


def swap(value):
    return shift(value, CORE, 1)


def spread_kernel(a_ref, b_ref, c_ref, out_ref):
    for copy in range(16):
        for member, ref in enumerate((a_ref, b_ref, c_ref)):
            out_ref[copy, :, pl.ds(member * 256, 256)] = ref[...]


def spread(a, b, c):
    return pl.pallas_call(
        spread_kernel,
        out_shape=jax.ShapeDtypeStruct((16, 64, 768), jnp.bfloat16),
        in_specs=[vmem()] * 3,
        out_specs=vmem(),
        name="spread",
    )(a, b, c)


def split_lanes(grad, first, keep_ref, send_ref, rows, start):
    for pair in range(grad.shape[1] // 256):
        left = grad[:, pair * 256 : pair * 256 + 128]
        right = grad[:, pair * 256 + 128 : pair * 256 + 256]
        low_half = lax.broadcasted_iota(jnp.int32, left.shape, 1) < 64
        turned = pltpu.roll(jnp.where(low_half, right, left), 64, 1)
        zero = jnp.where(low_half, left, turned)
        one = jnp.where(low_half, turned, right)
        columns = pl.ds(start + pair * 128, 128)
        keep_ref[rows, columns] = jnp.where(first, zero, one).astype(jnp.bfloat16)
        send_ref[rows, columns] = jnp.where(first, one, zero).astype(jnp.bfloat16)


TILE = 1024
TILES = 2048 // TILE


def grad_kernel(
    core_ref,
    k_ref,
    v_ref,
    h_ref,
    x_ref,
    o_ref,
    keep_ref,
    send_ref,
    narrow_ref,
    wide_ref,
    keep_buf,
    send_buf,
    narrow_sem,
    wide_sem,
    out_sem,
):
    narrow = [
        pltpu.make_async_copy(ref, narrow_ref.at[n], narrow_sem.at[n])
        for n, ref in enumerate((k_ref, v_ref, h_ref))
    ]
    wide = [
        pltpu.make_async_copy(
            ref.at[:, pl.ds(tile * TILE, TILE)],
            wide_ref.at[group, :, pl.ds(tile * TILE, TILE)],
            wide_sem.at[group * TILES + tile],
        )
        for group, ref in enumerate((x_ref, o_ref))
        for tile in range(TILES)
    ]
    narrow[0].start()
    wide[0].start()
    narrow[1].start()
    for copy in wide[1:TILES]:
        copy.start()
    narrow[2].start()
    for copy in wide[TILES:]:
        copy.start()
    first = core_ref[0] == 0
    outs = []
    for group, members in enumerate(((0, 1), (2,))):
        for tile in range(TILES):
            for member in members:
                if tile == 0:
                    narrow[member].wait()
                if member == members[0]:
                    wide[group * TILES + tile].wait()
                rows = pl.ds(member * 256, 256)
                grad = lax.dot_general(
                    narrow_ref[member],
                    wide_ref[group, :, pl.ds(tile * TILE, TILE)],
                    (((0,), (0,)), ((), ())),
                    preferred_element_type=jnp.float32,
                )
                split_lanes(grad, first, keep_buf, send_buf, rows, tile * TILE // 2)
                if tile < TILES - 1:
                    continue
                for side, (buf, ref) in enumerate(((keep_buf, keep_ref), (send_buf, send_ref))):
                    copy = pltpu.make_async_copy(
                        buf.at[rows, :], ref.at[rows, :], out_sem.at[member * 2 + side]
                    )
                    copy.start()
                    outs.append(copy)
    for copy in outs:
        copy.wait()


def hbm_only(value):
    return pltpu.with_memory_space_constraint(value, pltpu.HBM)


def in_hbm():
    return pl.BlockSpec(memory_space=pltpu.HBM)


def grad_halves(core, key_cot, value_cot, h_saved, x_saved, out_cot):
    return pl.pallas_call(
        grad_kernel,
        out_shape=(
            pltpu.HBM((768, 1024), jnp.bfloat16),
            pltpu.HBM((768, 1024), jnp.bfloat16),
        ),
        in_specs=[smem()] + [in_hbm()] * 5,
        out_specs=(in_hbm(), in_hbm()),
        scratch_shapes=[
            pltpu.VMEM((3, 2048, 256), jnp.bfloat16),
            pltpu.VMEM((2, 2048, 2048), jnp.bfloat16),
            pltpu.VMEM((768, 1024), jnp.bfloat16),
            pltpu.VMEM((768, 1024), jnp.bfloat16),
            pltpu.SemaphoreType.DMA((3,)),
            pltpu.SemaphoreType.DMA((2 * TILES,)),
            pltpu.SemaphoreType.DMA((6,)),
        ],
        compiler_params=pltpu.CompilerParams(vmem_limit_bytes=48 * MIB),
        name="grads",
    )(core, *[hbm_only(a) for a in (key_cot, value_cot, h_saved, x_saved, out_cot)])


def pair_kernel(keep_ref, recv_ref, parts_ref, keep_buf, sem):
    copies = []
    for member in range(3):
        rows = pl.ds(member * 256, 256)
        copies.append(
            pltpu.make_async_copy(keep_ref.at[rows, :], keep_buf.at[rows, :], sem.at[member])
        )
        copies[member].start()
    for member in range(3):
        rows = pl.ds(member * 256, 256)
        copies[member].wait()
        grad = keep_buf[rows, :].astype(jnp.float32) + recv_ref[rows, :].astype(jnp.float32)
        parts_ref[member] = grad.astype(jnp.bfloat16)


def pair_sum(keep, recv):
    return pl.pallas_call(
        pair_kernel,
        out_shape=jax.ShapeDtypeStruct((3, 256, 1024), jnp.bfloat16),
        in_specs=[in_hbm(), vmem()],
        out_specs=vmem(),
        scratch_shapes=[
            pltpu.VMEM((768, 1024), jnp.bfloat16),
            pltpu.SemaphoreType.DMA((3,)),
        ],
        compiler_params=pltpu.CompilerParams(vmem_limit_bytes=12 * MIB),
        name="pair_sum",
    )(hbm_only(keep), recv)


def project_kernel(core_ref, parts_ref, p_ref, mine_ref, other_ref, other_buf, sem):
    first = core_ref[0] == 0
    tiles = []
    upper = lax.broadcasted_iota(jnp.int32, (16, 2, 8, 128), 2) < 4
    copies = []
    for member in range(3):
        both = jnp.dot(
            parts_ref[member],
            p_ref[:, pl.ds(member * 256, 256)],
            preferred_element_type=jnp.float32,
        )
        turned = both.T
        for lanes in range(2):
            tiles.append(turned[:, lanes * 128 : (lanes + 1) * 128].reshape(16, 2, 8, 128))
        if member == 0:
            continue
        half = member - 1
        one, two, shared = tiles[3 * half : 3 * half + 3]
        for side, whole in enumerate((one, two)):
            part = shared if side == 0 else pltpu.roll(shared, 4, 2)
            piece = jnp.concatenate([whole, jnp.where(upper, part, 0.0)], axis=2)
            mine_ref[:, 2 * half + side] = jnp.where(first, piece[:, 0], piece[:, 1])
            other_buf[half, :, side] = jnp.where(first, piece[:, 1], piece[:, 0]).astype(
                jnp.bfloat16
            )
        copy = pltpu.make_async_copy(
            other_buf.at[half], other_ref.at[:, pl.ds(2 * half, 2)], sem.at[half]
        )
        copy.start()
        copies.append(copy)
    for copy in copies:
        copy.wait()


def project(core, parts, factors):
    return pl.pallas_call(
        project_kernel,
        out_shape=(
            jax.ShapeDtypeStruct((16, 4, 16, 128), jnp.float32),
            pltpu.HBM((16, 4, 16, 128), jnp.bfloat16),
        ),
        in_specs=[smem(), vmem(), vmem()],
        out_specs=(vmem(), in_hbm()),
        scratch_shapes=[
            pltpu.VMEM((2, 16, 2, 16, 128), jnp.bfloat16),
            pltpu.SemaphoreType.DMA((2,)),
        ],
        compiler_params=pltpu.CompilerParams(vmem_limit_bytes=12 * MIB),
        name="project",
    )(core, parts, factors)


def reduce_kernel(pieces_ref, out_ref):
    own = jnp.sum(pieces_ref[...].astype(jnp.float32), axis=0)
    total = jnp.sum(own * own)
    high = total.astype(jnp.bfloat16).astype(jnp.float32)
    row = lax.broadcasted_iota(jnp.int32, own.shape, 1)
    lane = lax.broadcasted_iota(jnp.int32, own.shape, 2)
    tail = jnp.where(row == 12, high, total - high)
    value = jnp.where(row < 12, own, jnp.where((lane == 0) & (row < 14), tail, 0.0))
    out_ref[...] = jnp.broadcast_to(value.astype(jnp.bfloat16)[None], out_ref.shape)


def reduce_pieces(pieces):
    return pl.pallas_call(
        reduce_kernel,
        out_shape=jax.ShapeDtypeStruct((16, 4, 16, 128), jnp.bfloat16),
        in_specs=[vmem()],
        out_specs=vmem(),
        compiler_params=pltpu.CompilerParams(vmem_limit_bytes=8 * MIB),
        name="reduce_pieces",
    )(pieces)


def direction_of(proj, m_one, m_two, inverse):
    normed = proj * inverse
    first = beta_one * m_one + (1 - beta_one) * normed
    second = beta_two * m_two + (1 - beta_two) * normed * normed
    return first, second, (first * lax.rsqrt(second)).astype(jnp.bfloat16)


ORDER = (0, 3, 1, 2)


def finish_kernel(*refs):
    place_ref, *piece_refs = refs[:3]
    refs = refs[1:]
    p_refs = refs[2:4]
    wm_refs = (refs[4:9], refs[9:14])
    p_own_refs = refs[14:17]
    m_refs = refs[17:20]
    step_refs = refs[20:23]
    copy_refs = refs[23:26]
    new_m_refs = refs[26:29]
    proj_ref, dir_ref, p_buf, wm_buf, p_own_buf, m_buf, turn_buf = refs[29:36]
    out_bufs = refs[36:39]
    whole_ref, moment_buf, step_buf, level_ref = refs[39:43]
    p_sem, wm_sem, small_sem, out_sem = refs[43:]
    z, y, core = place_ref[0], place_ref[1], place_ref[2]
    slots = (core, 1 - core)
    mine = (z * 4 + y) * 2 + core
    levels = [lax.rem(z + d, 4) for d in ORDER]
    columns = [lax.rem(y + d, 4) for d in ORDER]

    for index in range(4):
        level_ref[index] = levels[index]

    def wm_copy(side, array, turned):
        parts = pl.ds(0, 4) if array < 3 else pl.ds(0, 2) if array == 3 else pl.ds(2, 2)
        lead = min(array, 3)
        buf = wm_buf.at[side, parts, lead] if turned else wm_buf.at[side, lead, parts]
        return pltpu.make_async_copy(wm_refs[side][array], buf, wm_sem.at[side * 5 + array])

    for turned in (False, True):

        @pl.when((core == 1) == turned)
        def _():
            for array in range(5):
                wm_copy(0, array, turned).start()
                wm_copy(1, array, not turned).start()

    small = []
    for member in range(3):
        for refs_of, buf, sem in ((m_refs, m_buf, member), (p_own_refs, p_own_buf, 3 + member)):
            copy = pltpu.make_async_copy(refs_of[member], buf.at[member], small_sem.at[sem])
            copy.start()
            small.append(copy)
    p_copy = pltpu.make_async_copy(p_refs[1], p_buf, p_sem.at[0])
    p_copy.start()

    squares = jnp.zeros((8, 128), jnp.float32)
    upper = lax.broadcasted_iota(jnp.int32, (16, 8, 128), 1) < 4
    for half in range(2):
        for slot, pieces_ref in zip(slots, piece_refs):
            one = pieces_ref[:, 2 * half].astype(jnp.float32)
            two = pieces_ref[:, 2 * half + 1].astype(jnp.float32)
            tails = jnp.where(upper, 0.0, one[:, 8:] + two[:, 8:])
            squares = squares + jnp.sum(tails, axis=0)
            shared = jnp.where(upper, one[:, 8:], pltpu.roll(two[:, 8:], 4, 1))
            for tile, value in enumerate((one[:, :8], two[:, :8], shared)):
                lanes = pl.ds((3 * half + tile) * 128, 128)
                for index in range(16):
                    proj_ref[index * 2 + slot, :, lanes] = value[index]
    total = jnp.sum(squares)
    inverse = lax.rsqrt(jnp.full((8, 768), total / 786432 + 1e-06))

    for array in range(5):
        for side in range(2):
            wm_copy(side, array, False).wait()

    @pl.loop(0, 4)
    def _(turn):
        for side in range(2):
            for index in range(4):
                row = (level_ref[turn] * 4 + columns[index]) * 2 + slots[side]
                dir_ref[row] = direction_of(
                    proj_ref[row],
                    wm_buf[side, turn, index, 64:72].astype(jnp.float32),
                    wm_buf[side, turn, index, 72:80].astype(jnp.float32),
                    inverse,
                )[2].astype(jnp.float32)

    for member in range(3):
        cols = pl.ds(member * 256, 256)
        whole_ref[member] = dir_ref[:, :, cols].reshape(256, 256).astype(jnp.bfloat16)
    for copy in small:
        copy.wait()
    small_outs = []
    for member in range(3):
        cols = pl.ds(member * 256, 256)
        first, second, _ = direction_of(
            proj_ref[mine, :, cols], m_buf[member, 0], m_buf[member, 1], inverse[:, :256]
        )
        moment_buf[member, 0] = first
        moment_buf[member, 1] = second
        step_buf[member] = jnp.dot(
            p_own_buf[member], whole_ref[member], preferred_element_type=jnp.float32
        )
        for index, (buf, target) in enumerate(
            ((moment_buf, new_m_refs[member]), (step_buf, step_refs[member]))
        ):
            copy = pltpu.make_async_copy(
                buf.at[member], target, small_sem.at[6 + member * 2 + index]
            )
            copy.start()
            small_outs.append(copy)
    p_copy.wait()

    def out_copy(turn, level, member):
        if member < 2:
            part = pl.ds(level * 4, 4)
            source, target = out_bufs[member].at[part], copy_refs[member].at[part]
        else:
            part = pl.ds(pl.multiple_of(level * 512, 512), 512)
            source, target = out_bufs[2].at[:, part], copy_refs[2].at[:, part]
        return pltpu.make_async_copy(source, target, out_sem.at[turn * 3 + member])

    @pl.loop(0, 4)
    def _(turn):
        level = level_ref[turn]
        places = [level * 4 + column for column in columns]
        for member in range(3):
            cols = pl.ds(member * 256, 256)
            for side, p_ref in enumerate((p_refs[0], p_buf)):
                factor = jnp.concatenate([p_ref[place, :, cols] for place in places], axis=0)
                step = jnp.dot(
                    factor, whole_ref[member], preferred_element_type=jnp.float32
                ).reshape(4, 64, 256)
                weight = wm_buf[side, turn, :, :64, cols].astype(jnp.float32)
                fresh = (weight - learn_rate * step).astype(jnp.bfloat16)
                target = out_bufs[member] if member < 2 else turn_buf
                for index, place in enumerate(places):
                    target[place, slots[side]] = fresh[index]
            if member == 2:
                for index in range(4):
                    place = level * 4 + index
                    lanes = pl.ds(pl.multiple_of(place * 128, 128), 128)
                    out_bufs[2][:, lanes] = turn_buf[place].reshape(128, 256).T
            out_copy(turn, level, member).start()

    for copy in small_outs:
        copy.wait()
    for turn in range(4):
        for member in range(3):
            out_copy(turn, level_ref[turn], member).wait()


def finish(place, pieces, others, p_a, p_b, wm_a, wm_b, p_own, moments):
    rows = pltpu.HBM((16, 2, 64, 256), jnp.bfloat16)
    turned = pltpu.HBM((256, 2048), jnp.bfloat16)
    step = pltpu.HBM((64, 256), jnp.float32)
    moment = pltpu.HBM((2, 8, 256), jnp.float32)
    fetched = [hbm_only(a) for a in (p_b, *wm_a, *wm_b, *p_own, *moments)]
    return pl.pallas_call(
        finish_kernel,
        out_shape=(step,) * 3 + (rows, rows, turned) + (moment,) * 3,
        in_specs=[smem(), vmem(), vmem(), vmem()] + [in_hbm()] * len(fetched),
        out_specs=(in_hbm(),) * 9,
        scratch_shapes=[
            pltpu.VMEM((32, 8, 768), jnp.float32),
            pltpu.VMEM((32, 8, 768), jnp.float32),
            pltpu.VMEM((16, 64, 768), jnp.bfloat16),
            pltpu.VMEM((2, 4, 4, 80, 768), jnp.bfloat16),
            pltpu.VMEM((3, 64, 256), jnp.bfloat16),
            pltpu.VMEM((3, 2, 8, 256), jnp.float32),
            pltpu.VMEM((16, 2, 64, 256), jnp.bfloat16),
            pltpu.VMEM((16, 2, 64, 256), jnp.bfloat16),
            pltpu.VMEM((16, 2, 64, 256), jnp.bfloat16),
            pltpu.VMEM((256, 2048), jnp.bfloat16),
            pltpu.VMEM((3, 256, 256), jnp.bfloat16),
            pltpu.VMEM((3, 2, 8, 256), jnp.float32),
            pltpu.VMEM((3, 64, 256), jnp.float32),
            pltpu.SMEM((4,), jnp.int32),
            pltpu.SemaphoreType.DMA((1,)),
            pltpu.SemaphoreType.DMA((10,)),
            pltpu.SemaphoreType.DMA((12,)),
            pltpu.SemaphoreType.DMA((12,)),
        ],
        compiler_params=pltpu.CompilerParams(vmem_limit_bytes=32 * MIB),
        name="finish",
    )(place, pieces, others, p_a, *fetched)


def body(
    x_saved,
    h_saved,
    key_cot,
    value_cot,
    out_cot,
    w_key,
    w_value,
    w_out,
    p_key,
    p_value,
    p_out,
    m_key,
    m_value,
    m_out,
):
    place = jnp.stack([lax.axis_index(a) for a in FS]).astype(jnp.int32)
    core = place[2:]
    p_all = spread(p_key, p_value, p_out)
    p_a = lax.all_to_all(p_all, FAR, 0, 0, tiled=True)

    keep, send = grad_halves(core, key_cot, value_cot, h_saved, x_saved, out_cot)
    recv = swap(send)

    w_own = jnp.concatenate([w_key, w_value, w_out.T], axis=1)
    m_own = jnp.concatenate([m_key, m_value, m_out], axis=2).reshape(16, 768)
    wm_own = jnp.concatenate([w_own, m_own], axis=0).astype(jnp.bfloat16)
    line = [wm_own] + [crossed(wm_own, 0, by) for by in (1, -1, 2)]
    line = jnp.stack(line)

    parts = pair_sum(keep, recv)
    mine, other = project(core, parts, p_a.reshape(1024, 768))
    partial = (mine + swap(other).astype(jnp.float32)).astype(jnp.bfloat16)
    pieces = lax.all_to_all(
        partial.reshape(64, 16, 128), (*FAR, "tp"), 0, 0, tiled=True
    )
    near = crossed(line, 1, 1)
    after = crossed(line, 1, -1)
    p_b = swap(p_a)

    packed = reduce_pieces(pieces.reshape(16, 4, 16, 128))
    whole = lax.all_to_all(packed.reshape(64, 16, 128), (*FAR, "tp"), 0, 0, tiled=True)
    whole = whole.reshape(16, 4, 16, 128)
    others = swap(whole)
    far_one = crossed(near[:2], 1, 1)
    far_two = crossed(after[2:], 1, -1)
    wm_a = (line, near, after, far_one, far_two)
    wm_b = [swap(a) for a in wm_a[:3]]
    wm_b += [swap(a) for a in wm_a[3:]]
    outs = finish(
        place,
        whole,
        others,
        p_a,
        p_b,
        wm_a,
        wm_b,
        (p_key, p_value, p_out),
        (m_key, m_value, m_out),
    )
    return (
        outs[0],
        outs[1],
        outs[2].T,
        outs[3].reshape(2048, 256),
        outs[4].reshape(2048, 256),
        *outs[5:],
    )


def solution(mesh):
    split = Mesh(mesh.devices.reshape(4, 4, 2, mesh.shape["tp"]), ("fs_0", "fs_1", "fs_2", "tp"))
    in_specs = (
        P(FS, None),
        P(FS, "tp"),
        P(FS, "tp"),
        P(FS, "tp"),
        P(FS, None),
        P(FS, "tp"),
        P(FS, "tp"),
        P("tp", FS),
        P(FS, None),
        P(FS, None),
        P(FS, None),
        P(None, FS, "tp"),
        P(None, FS, "tp"),
        P(None, FS, "tp"),
    )
    out_specs = (
        P(FS, "tp"),
        P(FS, "tp"),
        P("tp", FS),
        P(None, "tp"),
        P(None, "tp"),
        P("tp", None),
        P(None, FS, "tp"),
        P(None, FS, "tp"),
        P(None, FS, "tp"),
    )
    return jax.shard_map(body, mesh=split, in_specs=in_specs, out_specs=out_specs, check_vma=False)
```

profile of v0, /device:TPU:1, one launch (start us, length us, event | category | flops | bytes accessed | tf_op | source)
XLA Modules:
  0.0 92.8 jit_solution(11712583020579386251)
XLA Ops:
  0.6 2.1 %spread.1 = bf16[16,64,768]{2,1,0:T(8,128)(2,1)} custom-call(bf16[64,256]{1,0:T(8,128)(2,1)} %refs_15_.1, bf16[64,256]{1,0:T(8,128)(2,1)} %refs_16_.1, bf16[64,256]{1,0:T(8,128)(2,1)} %refs_17_.1), custom_call_target="tpu_custom_call" | custom-call | tf_op jit(solution)/shard_map/spread/pallas_call | solution.py:56
  2.7 8.6 %all-to-all-start = ((bf16[16,64,768]{2,1,0:T(8,128)(2,1)}), bf16[16,64,768]{2,1,0:T(8,128)(2,1)S(1)}, u32[]{:S(2)}, u32[]{:S(2)}) async-start(bf16[16,64,768]{2,1,0:T(8,128)(2,1)} %spread.1), calls=%async_computation | async-start | bytes 3145728 | tf_op jit(solution)/shard_map/all_to_all | solution.py:492
  11.3 0.0 copy-start.7
  11.3 0.0 copy-start.8
  11.3 0.0 copy-start.9
  11.4 0.0 copy-start.3
  11.4 0.0 copy-start.4
  11.4 0.0 copy-start.5
  11.4 11.7 %grads.1 = (bf16[768,1024]{1,0:T(8,128)(2,1)}, bf16[768,1024]{1,0:T(8,128)(2,1)}) custom-call(s32[1]{0:T(128)} %bitcast.2.core_ref, bf16[2048,256]{1,0:T(8,128)(2,1)} %k_ref.1, bf16[2048,256]{1,0:T(8,128)(2,1)} %v_ref.1, bf16[2048,256]{1,0:T(8,128)(2,1)} %h_ref.1, bf16[2048,2048]{1,0:T(8,128)(2,1)} %x_ref.1, bf16[2048,2048]{1,0:T(8,128)(2,1)} %o_ref.1), custom_call_target="tpu_custom_call" | custom-call | tf_op jit(solution)/shard_map/grads/pallas_call | solution.py:158
  23.1 1.0 %collective-permute-start = (bf16[768,1024]{1,0:T(8,128)(2,1)}, bf16[768,1024]{1,0:T(8,128)(2,1)S(1)}, u32[]{:S(2)}, u32[]{:S(2)}) collective-permute-start(bf16[768,1024]{1,0:T(8,128)(2,1)} %get-tuple-element.23), channel_id=1, source_target_pairs={{0,4},{4,0},{1,5},{5,1},{2,6},{6,2},{3,7},{7,3},{8,12},{12,8},{9,1... | collective-permute-start | bytes 4718600 | tf_op jit(solution)/shard_map/ppermute | solution.py:29
  24.1 0.0 copy-done.7
  24.1 0.0 copy-done.8
  24.1 0.0 copy-done.9
  24.1 0.0 copy-done.3
  24.1 0.0 copy-done.4
  24.1 0.0 copy-done.5
  24.2 10.2 %all-to-all-done.refs_3_ = bf16[16,64,768]{2,1,0:T(8,128)(2,1)S(1)} async-done(((bf16[16,64,768]{2,1,0:T(8,128)(2,1)}), bf16[16,64,768]{2,1,0:T(8,128)(2,1)S(1)}, u32[]{:S(2)}, u32[]{:S(2)}) %all-to-all-start) | async-done | bytes 1572896 | tf_op jit(solution)/shard_map/all_to_all | solution.py:492
  34.4 2.4 %collective-permute-start.3 = (bf16[16,64,768]{2,1,0:T(8,128)(2,1)S(1)}, bf16[16,64,768]{2,1,0:T(8,128)(2,1)}, u32[]{:S(2)}, u32[]{:S(2)}) collective-permute-start(bf16[16,64,768]{2,1,0:T(8,128)(2,1)S(1)} %all-to-all-done.refs_3_), channel_id=1, source_target_pairs={{0,4},{4,0},{1,5},{5,1},{2,6},{6,2},{3,7},{7,3},{8,12},{12,8},{9,1... | collective-permute-start | bytes 4718600 | tf_op jit(solution)/shard_map/ppermute | solution.py:29
  36.8 0.1 collective-permute-start.4
  36.9 2.7 %collective-permute-start.5 = (bf16[80,768]{1,0:T(8,128)(2,1)S(1)}, bf16[80,768]{1,0:T(8,128)(2,1)S(1)}, u32[]{:S(2)}, u32[]{:S(2)}) collective-permute-start(bf16[80,768]{1,0:T(8,128)(2,1)S(1)} %pad_maximum_fusion.1), channel_id=1, source_target_pairs={{0,24},{4,100},{8,0},{12,108},{16,8},{20,116},{24,16},{28,124},{32... | collective-permute-start | bytes 368648 | tf_op jit(solution)/shard_map/ppermute | solution.py:42
  39.6 0.0 collective-permute-start.6
  39.6 0.0 collective-permute-done.recv_ref
  39.6 1.5 %pair_sum.1.parts_ref = bf16[3,256,1024]{2,1,0:T(8,128)(2,1)S(1)} custom-call(bf16[768,1024]{1,0:T(8,128)(2,1)} %get-tuple-element.22.keep_ref, bf16[768,1024]{1,0:T(8,128)(2,1)S(1)} %collective-permute-done.recv_ref), custom_call_target="tpu_custom_call" | custom-call | tf_op jit(solution)/shard_map/pair_sum/pallas_call | solution.py:196
  41.1 1.4 %project.1 = (f32[16,4,16,128]{3,2,1,0:T(8,128)S(1)}, bf16[16,4,16,128]{3,2,1,0:T(8,128)(2,1)}) custom-call(s32[1]{0:T(128)} %bitcast.2.core_ref, bf16[3,256,1024]{2,1,0:T(8,128)(2,1)S(1)} %pair_sum.1.parts_ref, bf16[1024,768]{1,0:T(8,128)(2,1)S(1)} %bitcast.21), custom_call_target="tpu_custom_call" | custom-call | tf_op jit(solution)/shard_map/project/pallas_call | solution.py:245
  42.5 0.6 collective-permute-start.1
  43.2 0.0 collective-permute-done.4
  43.2 0.0 collective-permute-done.5
  43.2 1.9 %collective-permute-done.6 = bf16[80,768]{1,0:T(8,128)(2,1)S(1)} collective-permute-done((bf16[80,768]{1,0:T(8,128)(2,1)S(1)}, bf16[80,768]{1,0:T(8,128)(2,1)S(1)}, u32[]{:S(2)}, u32[]{:S(2)}) %collective-permute-start.6) | collective-permute-done | bytes 122912 | tf_op jit(solution)/shard_map/ppermute | solution.py:42
  45.1 0.0 copy-start
  45.1 0.1 collective-permute-start.7
  45.2 2.7 %collective-permute-start.8 = (bf16[4,80,768]{2,1,0:T(8,128)(2,1)S(1)}, bf16[4,80,768]{2,1,0:T(8,128)(2,1)}, u32[]{:S(2)}, u32[]{:S(2)}) collective-permute-start(bf16[4,80,768]{2,1,0:T(8,128)(2,1)S(1)} %pad_maximum_fusion.refs_5_), channel_id=1, source_target_pairs={{0,96},{4,28},{8,104},{12,4},{16,112},{20,12},{24,120},{28,20},{32... | collective-permute-start | bytes 1474568 | tf_op jit(solution)/shard_map/ppermute | solution.py:42
  47.9 2.0 %collective-permute-start.11 = (bf16[4,80,768]{2,1,0:T(8,128)(2,1)S(1)}, bf16[4,80,768]{2,1,0:T(8,128)(2,1)}, u32[]{:S(2)}, u32[]{:S(2)}) collective-permute-start(bf16[4,80,768]{2,1,0:T(8,128)(2,1)S(1)} %pad_maximum_fusion.refs_5_), channel_id=1, source_target_pairs={{0,4},{4,0},{1,5},{5,1},{2,6},{6,2},{3,7},{7,3},{8,12},{12,8},{9,1... | collective-permute-start | bytes 1474568 | tf_op jit(solution)/shard_map/ppermute | solution.py:29
  49.9 0.0 collective-permute-done.1
  49.9 0.8 add_convert_fusion
  50.6 5.7 %all-to-all-start.1 = ((bf16[64,16,128]{2,1,0:T(8,128)(2,1)}), bf16[64,16,128]{2,1,0:T(8,128)(2,1)S(1)}, u32[]{:S(2)}, u32[]{:S(2)}) async-start(bf16[64,16,128]{2,1,0:T(8,128)(2,1)} %bitcast.4), calls=%async_computation.1 | async-start | bytes 524288 | tf_op jit(solution)/shard_map/all_to_all | solution.py:506
  56.3 0.0 collective-permute-done.7.refs_6_
  56.3 0.0 copy-start.1
  56.3 0.4 collective-permute-start.12
  56.7 9.5 %all-to-all-done.1 = bf16[64,16,128]{2,1,0:T(8,128)(2,1)S(1)} async-done(((bf16[64,16,128]{2,1,0:T(8,128)(2,1)}), bf16[64,16,128]{2,1,0:T(8,128)(2,1)S(1)}, u32[]{:S(2)}, u32[]{:S(2)}) %all-to-all-start.1) | async-done | bytes 262176 | tf_op jit(solution)/shard_map/all_to_all | solution.py:506
  66.2 0.9 reduce_pieces.1
  67.1 4.7 %all-to-all-start.2 = ((bf16[64,16,128]{2,1,0:T(8,128)(2,1)}), bf16[64,16,128]{2,1,0:T(8,128)(2,1)S(1)}, u32[]{:S(2)}, u32[]{:S(2)}) async-start(bf16[64,16,128]{2,1,0:T(8,128)(2,1)} %bitcast.6), calls=%async_computation.2 | async-start | bytes 524288 | tf_op jit(solution)/shard_map/all_to_all | solution.py:514
  71.9 1.1 %collective-permute-start.9 = (bf16[2,80,768]{2,1,0:T(8,128)(2,1)S(1)}, bf16[2,80,768]{2,1,0:T(8,128)(2,1)S(1)}, u32[]{:S(2)}, u32[]{:S(2)}) collective-permute-start(bf16[2,80,768]{2,1,0:T(8,128)(2,1)S(1)} %slice.8), channel_id=1, source_target_pairs={{0,32},{4,12},{8,40},{12,20},{16,48},{20,28},{24,56},{28,4},{32,64... | collective-permute-start | bytes 737288 | tf_op jit(solution)/shard_map/ppermute | solution.py:42
  73.0 0.0 collective-permute-done.8.refs_7_
  73.0 1.7 %slice.9 = bf16[2,80,768]{2,1,0:T(8,128)(2,1)} slice(bf16[4,80,768]{2,1,0:T(8,128)(2,1)} %collective-permute-done.8.refs_7_), slice={[2:4], [0:80], [0:768]} | slice | bytes 491520 | tf_op jit(solution)/shard_map/slice | solution.py:518
  74.6 0.0 copy-done
  74.6 1.7 %collective-permute-start.10 = (bf16[2,80,768]{2,1,0:T(8,128)(2,1)}, bf16[2,80,768]{2,1,0:T(8,128)(2,1)}, u32[]{:S(2)}, u32[]{:S(2)}) collective-permute-start(bf16[2,80,768]{2,1,0:T(8,128)(2,1)} %slice.9), channel_id=1, source_target_pairs={{0,96},{4,28},{8,104},{12,4},{16,112},{20,12},{24,120},{28,20},{32... | collective-permute-start | bytes 737288 | tf_op jit(solution)/shard_map/ppermute | solution.py:42
  76.3 0.0 collective-permute-done.11.refs_10_
  76.3 2.2 %collective-permute-start.13 = (bf16[4,80,768]{2,1,0:T(8,128)(2,1)}, bf16[4,80,768]{2,1,0:T(8,128)(2,1)S(1)}, u32[]{:S(2)}, u32[]{:S(2)}) collective-permute-start(bf16[4,80,768]{2,1,0:T(8,128)(2,1)} %collective-permute-done.8.refs_7_), channel_id=1, source_target_pairs={{0,4},{4,0},{1,5},{5,1},{2,6},{6,2},{3,7},{7,3},{8,12},{12,8},{9,1... | collective-permute-start | bytes 1474568 | tf_op jit(solution)/shard_map/ppermute | solution.py:29
  78.4 2.4 %collective-permute-done.9.refs_8_ = bf16[2,80,768]{2,1,0:T(8,128)(2,1)S(1)} collective-permute-done((bf16[2,80,768]{2,1,0:T(8,128)(2,1)S(1)}, bf16[2,80,768]{2,1,0:T(8,128)(2,1)S(1)}, u32[]{:S(2)}, u32[]{:S(2)}) %collective-permute-start.9) | collective-permute-done | bytes 245792 | tf_op jit(solution)/shard_map/ppermute | solution.py:42
  80.8 0.5 all-to-all-done.2
  81.4 2.7 %collective-permute-start.2 = (bf16[16,4,16,128]{3,2,1,0:T(8,128)(2,1)S(1)}, bf16[16,4,16,128]{3,2,1,0:T(8,128)(2,1)S(1)}, u32[]{:S(2)}, u32[]{:S(2)}) collective-permute-start(bf16[16,4,16,128]{3,2,1,0:T(8,128)(2,1)S(1)} %bitcast.22), channel_id=1, source_target_pairs={{0,4},{4,0},{1,5},{5,1},{2,6},{6,2},{3,7},{7,3},{8,12},{12,8},{9,1... | collective-permute-start | bytes 786440 | tf_op jit(solution)/shard_map/ppermute | solution.py:29
  84.1 0.0 collective-permute-done.10.refs_9_
  84.1 0.0 collective-permute-start.14
  84.1 0.0 collective-permute-done.12.refs_11_
  84.1 0.5 collective-permute-start.15
  84.6 0.1 pad_add_fusion.refs_0_
  84.7 0.0 collective-permute-done.13.refs_12_
  84.7 1.0 %collective-permute-done.14.refs_13_ = bf16[2,80,768]{2,1,0:T(8,128)(2,1)} collective-permute-done((bf16[2,80,768]{2,1,0:T(8,128)(2,1)S(1)}, bf16[2,80,768]{2,1,0:T(8,128)(2,1)}, u32[]{:S(2)}, u32[]{:S(2)}) %collective-permute-start.14) | collective-permute-done | bytes 245792 | tf_op jit(solution)/shard_map/ppermute | solution.py:29
  85.7 0.4 collective-permute-done.15.refs_14_
  86.1 0.0 collective-permute-done.2.refs_2_
  86.1 0.0 collective-permute-done.3.refs_4_
  86.1 0.0 copy-done.1
  86.1 0.0 copy-done.6
  86.1 6.6 %finish.1 = (f32[64,256]{1,0:T(8,128)}, f32[64,256]{1,0:T(8,128)}, f32[64,256]{1,0:T(8,128)}, bf16[16,2,64,256]{3,2,1,0:T(8,128)(2,1)}, bf16[16,2,64,256]{3,2,1,...) custom-call(s32[3]{0:T(128)S(1)} %pad_add_fusion.refs_0_, ...), custom_call_target="tpu_custom_call" | custom-call | tf_op jit(solution)/shard_map/finish/pallas_call | solution.py:443
  (9 shorter events, 0.1 us)
Async XLA Ops:
  2.7 31.7 %all-to-all-start = ((bf16[16,64,768]{2,1,0:T(8,128)(2,1)}), bf16[16,64,768]{2,1,0:T(8,128)(2,1)S(1)}, u32[]{:S(2)}, u32[]{:S(2)}) async-start(bf16[16,64,768]{2,1,0:T(8,128)(2,1)} %spread.1), calls=%async_computation | async-start | bytes 3145728 | tf_op jit(solution)/shard_map/all_to_all | solution.py:492
  11.3 12.8 %copy-start.7 = (f32[2,8,256]{2,1,0:T(8,128)S(1)}, f32[2,8,256]{2,1,0:T(8,128)}, u32[]{:S(2)}) copy-start(f32[2,8,256]{2,1,0:T(8,128)} %refs_20_.1) | copy-start | bytes 49156
  11.3 12.8 %copy-start.8 = (f32[2,8,256]{2,1,0:T(8,128)S(1)}, f32[2,8,256]{2,1,0:T(8,128)}, u32[]{:S(2)}) copy-start(f32[2,8,256]{2,1,0:T(8,128)} %refs_19_.1) | copy-start | bytes 49156
  11.3 12.8 %copy-start.9 = (f32[2,8,256]{2,1,0:T(8,128)S(1)}, f32[2,8,256]{2,1,0:T(8,128)}, u32[]{:S(2)}) copy-start(f32[2,8,256]{2,1,0:T(8,128)} %refs_18_.1) | copy-start | bytes 49156
  11.4 12.8 %copy-start.3 = (f32[256,64]{0,1:T(8,128)S(1)}, f32[256,64]{0,1:T(8,128)}, u32[]{:S(2)}) copy-start(f32[256,64]{0,1:T(8,128)} %param.21) | copy-start | bytes 196612
  11.4 12.8 %copy-start.4 = (f32[64,256]{1,0:T(8,128)S(1)}, f32[64,256]{1,0:T(8,128)}, u32[]{:S(2)}) copy-start(f32[64,256]{1,0:T(8,128)} %param.20) | copy-start | bytes 196612
  11.4 12.8 %copy-start.5 = (f32[64,256]{1,0:T(8,128)S(1)}, f32[64,256]{1,0:T(8,128)}, u32[]{:S(2)}) copy-start(f32[64,256]{1,0:T(8,128)} %param.19) | copy-start | bytes 196612
  23.1 16.5 %collective-permute-start = (bf16[768,1024]{1,0:T(8,128)(2,1)}, bf16[768,1024]{1,0:T(8,128)(2,1)S(1)}, u32[]{:S(2)}, u32[]{:S(2)}) collective-permute-start(bf16[768,1024]{1,0:T(8,128)(2,1)} %get-tuple-element.23), channel_id=1, source_target_pairs={{0,4},{4,0},{1,5},{5,1},{2,6},{6,2},{3,7},{7,3},{8,12},{12,8},{9,1... | collective-permute-start | bytes 4718600 | tf_op jit(solution)/shard_map/ppermute | solution.py:29
  34.4 51.7 %collective-permute-start.3 = (bf16[16,64,768]{2,1,0:T(8,128)(2,1)S(1)}, bf16[16,64,768]{2,1,0:T(8,128)(2,1)}, u32[]{:S(2)}, u32[]{:S(2)}) collective-permute-start(bf16[16,64,768]{2,1,0:T(8,128)(2,1)S(1)} %all-to-all-done.refs_3_), channel_id=1, source_target_pairs={{0,4},{4,0},{1,5},{5,1},{2,6},{6,2},{3,7},{7,3},{8,12},{12,8},{9,1... | collective-permute-start | bytes 4718600 | tf_op jit(solution)/shard_map/ppermute | solution.py:29
  36.8 6.4 %collective-permute-start.4 = (bf16[80,768]{1,0:T(8,128)(2,1)S(1)}, bf16[80,768]{1,0:T(8,128)(2,1)S(1)}, u32[]{:S(2)}, u32[]{:S(2)}) collective-permute-start(bf16[80,768]{1,0:T(8,128)(2,1)S(1)} %pad_maximum_fusion.1), channel_id=1, source_target_pairs={{0,8},{4,36},{8,16},{12,44},{16,24},{20,52},{24,0},{28,60},{32,40}... | collective-permute-start | bytes 368648 | tf_op jit(solution)/shard_map/ppermute | solution.py:42
  36.9 6.3 %collective-permute-start.5 = (bf16[80,768]{1,0:T(8,128)(2,1)S(1)}, bf16[80,768]{1,0:T(8,128)(2,1)S(1)}, u32[]{:S(2)}, u32[]{:S(2)}) collective-permute-start(bf16[80,768]{1,0:T(8,128)(2,1)S(1)} %pad_maximum_fusion.1), channel_id=1, source_target_pairs={{0,24},{4,100},{8,0},{12,108},{16,8},{20,116},{24,16},{28,124},{32... | collective-permute-start | bytes 368648 | tf_op jit(solution)/shard_map/ppermute | solution.py:42
  39.6 5.5 %collective-permute-start.6 = (bf16[80,768]{1,0:T(8,128)(2,1)S(1)}, bf16[80,768]{1,0:T(8,128)(2,1)S(1)}, u32[]{:S(2)}, u32[]{:S(2)}) collective-permute-start(bf16[80,768]{1,0:T(8,128)(2,1)S(1)} %pad_maximum_fusion.1), channel_id=1, source_target_pairs={{0,16},{4,68},{8,24},{12,76},{16,0},{20,84},{24,8},{28,92},{32,48}... | collective-permute-start | bytes 368648 | tf_op jit(solution)/shard_map/ppermute | solution.py:42
  42.5 7.3 %collective-permute-start.1 = (bf16[16,4,16,128]{3,2,1,0:T(8,128)(2,1)}, bf16[16,4,16,128]{3,2,1,0:T(8,128)(2,1)S(1)}, u32[]{:S(2)}, u32[]{:S(2)}) collective-permute-start(bf16[16,4,16,128]{3,2,1,0:T(8,128)(2,1)} %get-tuple-element.25), channel_id=1, source_target_pairs={{0,4},{4,0},{1,5},{5,1},{2,6},{6,2},{3,7},{7,3},{8,12},{12,8},{9,1... | collective-permute-start | bytes 786440 | tf_op jit(solution)/shard_map/ppermute | solution.py:29
  45.1 29.5 %copy-start = (bf16[4,80,768]{2,1,0:T(8,128)(2,1)}, bf16[4,80,768]{2,1,0:T(8,128)(2,1)S(1)}, u32[]{:S(2)}) copy-start(bf16[4,80,768]{2,1,0:T(8,128)(2,1)S(1)} %pad_maximum_fusion.refs_5_) | copy-start | bytes 1474564
  45.1 11.2 %collective-permute-start.7 = (bf16[4,80,768]{2,1,0:T(8,128)(2,1)S(1)}, bf16[4,80,768]{2,1,0:T(8,128)(2,1)S(1)}, u32[]{:S(2)}, u32[]{:S(2)}) collective-permute-start(bf16[4,80,768]{2,1,0:T(8,128)(2,1)S(1)} %pad_maximum_fusion.refs_5_), channel_id=1, source_target_pairs={{0,32},{4,12},{8,40},{12,20},{16,48},{20,28},{24,56},{28,4},{32,64... | collective-permute-start | bytes 1474568 | tf_op jit(solution)/shard_map/ppermute | solution.py:42
  45.2 27.7 %collective-permute-start.8 = (bf16[4,80,768]{2,1,0:T(8,128)(2,1)S(1)}, bf16[4,80,768]{2,1,0:T(8,128)(2,1)}, u32[]{:S(2)}, u32[]{:S(2)}) collective-permute-start(bf16[4,80,768]{2,1,0:T(8,128)(2,1)S(1)} %pad_maximum_fusion.refs_5_), channel_id=1, source_target_pairs={{0,96},{4,28},{8,104},{12,4},{16,112},{20,12},{24,120},{28,20},{32... | collective-permute-start | bytes 1474568 | tf_op jit(solution)/shard_map/ppermute | solution.py:42
  47.9 28.4 %collective-permute-start.11 = (bf16[4,80,768]{2,1,0:T(8,128)(2,1)S(1)}, bf16[4,80,768]{2,1,0:T(8,128)(2,1)}, u32[]{:S(2)}, u32[]{:S(2)}) collective-permute-start(bf16[4,80,768]{2,1,0:T(8,128)(2,1)S(1)} %pad_maximum_fusion.refs_5_), channel_id=1, source_target_pairs={{0,4},{4,0},{1,5},{5,1},{2,6},{6,2},{3,7},{7,3},{8,12},{12,8},{9,1... | collective-permute-start | bytes 1474568 | tf_op jit(solution)/shard_map/ppermute | solution.py:29
  50.6 15.6 %all-to-all-start.1 = ((bf16[64,16,128]{2,1,0:T(8,128)(2,1)}), bf16[64,16,128]{2,1,0:T(8,128)(2,1)S(1)}, u32[]{:S(2)}, u32[]{:S(2)}) async-start(bf16[64,16,128]{2,1,0:T(8,128)(2,1)} %bitcast.4), calls=%async_computation.1 | async-start | bytes 524288 | tf_op jit(solution)/shard_map/all_to_all | solution.py:506
  56.3 29.7 %copy-start.1 = (bf16[4,80,768]{2,1,0:T(8,128)(2,1)}, bf16[4,80,768]{2,1,0:T(8,128)(2,1)S(1)}, u32[]{:S(2)}) copy-start(bf16[4,80,768]{2,1,0:T(8,128)(2,1)S(1)} %collective-permute-done.7.refs_6_) | copy-start | bytes 1474564
  56.3 27.7 %collective-permute-start.12 = (bf16[4,80,768]{2,1,0:T(8,128)(2,1)S(1)}, bf16[4,80,768]{2,1,0:T(8,128)(2,1)}, u32[]{:S(2)}, u32[]{:S(2)}) collective-permute-start(bf16[4,80,768]{2,1,0:T(8,128)(2,1)S(1)} %collective-permute-done.7.refs_6_), channel_id=1, source_target_pairs={{0,4},{4,0},{1,5},{5,1},{2,6},{6,2},{3,7},{7,3},{8,12},{12,8},{9,1... | collective-permute-start | bytes 1474568 | tf_op jit(solution)/shard_map/ppermute | solution.py:29
  67.1 14.2 %all-to-all-start.2 = ((bf16[64,16,128]{2,1,0:T(8,128)(2,1)}), bf16[64,16,128]{2,1,0:T(8,128)(2,1)S(1)}, u32[]{:S(2)}, u32[]{:S(2)}) async-start(bf16[64,16,128]{2,1,0:T(8,128)(2,1)} %bitcast.6), calls=%async_computation.2 | async-start | bytes 524288 | tf_op jit(solution)/shard_map/all_to_all | solution.py:514
  71.9 8.9 %collective-permute-start.9 = (bf16[2,80,768]{2,1,0:T(8,128)(2,1)S(1)}, bf16[2,80,768]{2,1,0:T(8,128)(2,1)S(1)}, u32[]{:S(2)}, u32[]{:S(2)}) collective-permute-start(bf16[2,80,768]{2,1,0:T(8,128)(2,1)S(1)} %slice.8), channel_id=1, source_target_pairs={{0,32},{4,12},{8,40},{12,20},{16,48},{20,28},{24,56},{28,4},{32,64... | collective-permute-start | bytes 737288 | tf_op jit(solution)/shard_map/ppermute | solution.py:42
  74.6 9.4 %collective-permute-start.10 = (bf16[2,80,768]{2,1,0:T(8,128)(2,1)}, bf16[2,80,768]{2,1,0:T(8,128)(2,1)}, u32[]{:S(2)}, u32[]{:S(2)}) collective-permute-start(bf16[2,80,768]{2,1,0:T(8,128)(2,1)} %slice.9), channel_id=1, source_target_pairs={{0,96},{4,28},{8,104},{12,4},{16,112},{20,12},{24,120},{28,20},{32... | collective-permute-start | bytes 737288 | tf_op jit(solution)/shard_map/ppermute | solution.py:42
  76.3 8.4 %collective-permute-start.13 = (bf16[4,80,768]{2,1,0:T(8,128)(2,1)}, bf16[4,80,768]{2,1,0:T(8,128)(2,1)S(1)}, u32[]{:S(2)}, u32[]{:S(2)}) collective-permute-start(bf16[4,80,768]{2,1,0:T(8,128)(2,1)} %collective-permute-done.8.refs_7_), channel_id=1, source_target_pairs={{0,4},{4,0},{1,5},{5,1},{2,6},{6,2},{3,7},{7,3},{8,12},{12,8},{9,1... | collective-permute-start | bytes 1474568 | tf_op jit(solution)/shard_map/ppermute | solution.py:29
  80.8 5.2 %copy-start.6 = (bf16[2,80,768]{2,1,0:T(8,128)(2,1)}, bf16[2,80,768]{2,1,0:T(8,128)(2,1)S(1)}, u32[]{:S(2)}) copy-start(bf16[2,80,768]{2,1,0:T(8,128)(2,1)S(1)} %collective-permute-done.9.refs_8_) | copy-start | bytes 737284
  81.4 4.7 %collective-permute-start.2 = (bf16[16,4,16,128]{3,2,1,0:T(8,128)(2,1)S(1)}, bf16[16,4,16,128]{3,2,1,0:T(8,128)(2,1)S(1)}, u32[]{:S(2)}, u32[]{:S(2)}) collective-permute-start(bf16[16,4,16,128]{3,2,1,0:T(8,128)(2,1)S(1)} %bitcast.22), channel_id=1, source_target_pairs={{0,4},{4,0},{1,5},{5,1},{2,6},{6,2},{3,7},{7,3},{8,12},{12,8},{9,1... | collective-permute-start | bytes 786440 | tf_op jit(solution)/shard_map/ppermute | solution.py:29
  84.1 1.6 %collective-permute-start.14 = (bf16[2,80,768]{2,1,0:T(8,128)(2,1)S(1)}, bf16[2,80,768]{2,1,0:T(8,128)(2,1)}, u32[]{:S(2)}, u32[]{:S(2)}) collective-permute-start(bf16[2,80,768]{2,1,0:T(8,128)(2,1)S(1)} %collective-permute-done.9.refs_8_), channel_id=1, source_target_pairs={{0,4},{4,0},{1,5},{5,1},{2,6},{6,2},{3,7},{7,3},{8,12},{12,8},{9,1... | collective-permute-start | bytes 737288 | tf_op jit(solution)/shard_map/ppermute | solution.py:29
  84.1 2.0 %collective-permute-start.15 = (bf16[2,80,768]{2,1,0:T(8,128)(2,1)}, bf16[2,80,768]{2,1,0:T(8,128)(2,1)}, u32[]{:S(2)}, u32[]{:S(2)}) collective-permute-start(bf16[2,80,768]{2,1,0:T(8,128)(2,1)} %collective-permute-done.10.refs_9_), channel_id=1, source_target_pairs={{0,4},{4,0},{1,5},{5,1},{2,6},{6,2},{3,7},{7,3},{8,12},{12,8},{9,1... | collective-permute-start | bytes 737288 | tf_op jit(solution)/shard_map/ppermute | solution.py:29
  84.7 1.4 %copy-start.2 = (bf16[4,80,768]{2,1,0:T(8,128)(2,1)}, bf16[4,80,768]{2,1,0:T(8,128)(2,1)S(1)}, u32[]{:S(2)}) copy-start(bf16[4,80,768]{2,1,0:T(8,128)(2,1)S(1)} %collective-permute-done.13.refs_12_) | copy-start | bytes 1474564
where the time goes:
time: 93.2 us; the launch traced here: 92.8 us
  starting transfers between devices  39 us (42%)
  waiting for transfers between devices  26 us (28%)
  Pallas kernels  24.1 us (26%)
  local copies, waits for them, and re-layouts  1.72 us (2%)
  between operations  1.05 us (1%)
    ppermute x9, starting transfers between devices, shift(): lax.ppermute(value, axis, [(i, (i + by) % size) for i in range(size)])  11.8 us
    pallas_call x1, Pallas kernels, grad_halves(): pl.pallas_call(grad_kernel, out_shape=(pltpu.HBM((768, 1024), jnp.bfloat1...  11.7 us
    all_to_all x1, waiting for transfers between devices, body(): p_a = lax.all_to_all(p_all, FAR, 0, 0, tiled=True)  10.2 us
    all_to_all x1, waiting for transfers between devices, body(): lax.all_to_all(partial.reshape(64, 16, 128), (*FAR, 'tp'), 0, 0, tiled=True)  9.52 us
    all_to_all x1, starting transfers between devices, body(): p_a = lax.all_to_all(p_all, FAR, 0, 0, tiled=True)  8.59 us
    ppermute x7, starting transfers between devices, crossed(): return lax.ppermute(value, FS, pairs)  8.22 us
    pallas_call x1, Pallas kernels, finish(): pl.pallas_call(finish_kernel, out_shape=(step,) * 3 + (rows, rows, turned...  6.55 us
    all_to_all x1, starting transfers between devices, body(): lax.all_to_all(partial.reshape(64, 16, 128), (*FAR, 'tp'), 0, 0, tiled=True)  5.67 us
  transfers between devices with their start and end apart: 19, of which 7 were waited for; matrix products, arithmetic and copies ran while one was open for 3% of the time, Pallas kernels for 17%

commit v1 on v0

--- a/solution.py
+++ b/solution.py
@@ -281,6 +281,25 @@
     )(pieces)
 
 
+def line_kernel(own_ref, below_ref, above_ref, across_ref, one_ref, two_ref):
+    one_ref[0] = own_ref[...]
+    one_ref[1] = below_ref[...]
+    two_ref[0] = above_ref[...]
+    two_ref[1] = across_ref[...]
+
+
+def join_line(*blocks):
+    half = jax.ShapeDtypeStruct((2, 80, 768), jnp.bfloat16)
+    return pl.pallas_call(
+        line_kernel,
+        out_shape=(half, half),
+        in_specs=[vmem()] * 4,
+        out_specs=(vmem(),) * 2,
+        compiler_params=pltpu.CompilerParams(vmem_limit_bytes=8 * MIB),
+        name="join_line",
+    )(*blocks)
+
+
 def direction_of(proj, m_one, m_two, inverse):
     normed = proj * inverse
     first = beta_one * m_one + (1 - beta_one) * normed
@@ -295,16 +314,16 @@
     place_ref, *piece_refs = refs[:3]
     refs = refs[1:]
     p_refs = refs[2:4]
-    wm_refs = (refs[4:9], refs[9:14])
-    p_own_refs = refs[14:17]
-    m_refs = refs[17:20]
-    step_refs = refs[20:23]
-    copy_refs = refs[23:26]
-    new_m_refs = refs[26:29]
-    proj_ref, dir_ref, p_buf, wm_buf, p_own_buf, m_buf, turn_buf = refs[29:36]
-    out_bufs = refs[36:39]
-    whole_ref, moment_buf, step_buf, level_ref = refs[39:43]
-    p_sem, wm_sem, small_sem, out_sem = refs[43:]
+    wm_refs = (refs[4:12], refs[12:20])
+    p_own_refs = refs[20:23]
+    m_refs = refs[23:26]
+    step_refs = refs[26:29]
+    copy_refs = refs[29:32]
+    new_m_refs = refs[32:35]
+    proj_ref, dir_ref, p_buf, wm_buf, p_own_buf, m_buf, turn_buf = refs[35:42]
+    out_bufs = refs[42:45]
+    whole_ref, moment_buf, step_buf, level_ref = refs[45:49]
+    p_sem, wm_sem, small_sem, out_sem = refs[49:]
     z, y, core = place_ref[0], place_ref[1], place_ref[2]
     slots = (core, 1 - core)
     mine = (z * 4 + y) * 2 + core
@@ -315,16 +334,15 @@
         level_ref[index] = levels[index]
 
     def wm_copy(side, array, turned):
-        parts = pl.ds(0, 4) if array < 3 else pl.ds(0, 2) if array == 3 else pl.ds(2, 2)
-        lead = min(array, 3)
+        parts, lead = pl.ds(array % 2 * 2, 2), array // 2
         buf = wm_buf.at[side, parts, lead] if turned else wm_buf.at[side, lead, parts]
-        return pltpu.make_async_copy(wm_refs[side][array], buf, wm_sem.at[side * 5 + array])
+        return pltpu.make_async_copy(wm_refs[side][array], buf, wm_sem.at[side * 8 + array])
 
     for turned in (False, True):
 
         @pl.when((core == 1) == turned)
         def _():
-            for array in range(5):
+            for array in range(8):
                 wm_copy(0, array, turned).start()
                 wm_copy(1, array, not turned).start()
 
@@ -353,7 +371,7 @@
     total = jnp.sum(squares)
     inverse = lax.rsqrt(jnp.full((8, 768), total / 786432 + 1e-06))
 
-    for array in range(5):
+    for array in range(8):
         for side in range(2):
             wm_copy(side, array, False).wait()
 
@@ -408,7 +426,7 @@
     def _(turn):
         level = level_ref[turn]
         places = [level * 4 + column for column in columns]
-        for member in range(3):
+        for member in (2, 0, 1):
             cols = pl.ds(member * 256, 256)
             for side, p_ref in enumerate((p_refs[0], p_buf)):
                 factor = jnp.concatenate([p_ref[place, :, cols] for place in places], axis=0)
@@ -461,7 +479,7 @@
             pltpu.VMEM((3, 64, 256), jnp.float32),
             pltpu.SMEM((4,), jnp.int32),
             pltpu.SemaphoreType.DMA((1,)),
-            pltpu.SemaphoreType.DMA((10,)),
+            pltpu.SemaphoreType.DMA((16,)),
             pltpu.SemaphoreType.DMA((12,)),
             pltpu.SemaphoreType.DMA((12,)),
         ],
@@ -497,8 +515,10 @@
     w_own = jnp.concatenate([w_key, w_value, w_out.T], axis=1)
     m_own = jnp.concatenate([m_key, m_value, m_out], axis=2).reshape(16, 768)
     wm_own = jnp.concatenate([w_own, m_own], axis=0).astype(jnp.bfloat16)
-    line = [wm_own] + [crossed(wm_own, 0, by) for by in (1, -1, 2)]
-    line = jnp.stack(line)
+    below = crossed(wm_own, 0, 1)
+    above = crossed(wm_own, 0, -1)
+    across = crossed(wm_own, 0, 2)
+    line_one, line_two = join_line(wm_own, below, above, across)
 
     parts = pair_sum(keep, recv)
     mine, other = project(core, parts, p_a.reshape(1024, 768))
@@ -506,19 +526,21 @@
     pieces = lax.all_to_all(
         partial.reshape(64, 16, 128), (*FAR, "tp"), 0, 0, tiled=True
     )
-    near = crossed(line, 1, 1)
-    after = crossed(line, 1, -1)
+    near_one = crossed(line_one, 1, 1)
+    after_two = crossed(line_two, 1, -1)
+    near_two = crossed(line_two, 1, 1)
+    after_one = crossed(line_one, 1, -1)
     p_b = swap(p_a)
 
     packed = reduce_pieces(pieces.reshape(16, 4, 16, 128))
     whole = lax.all_to_all(packed.reshape(64, 16, 128), (*FAR, "tp"), 0, 0, tiled=True)
     whole = whole.reshape(16, 4, 16, 128)
     others = swap(whole)
-    far_one = crossed(near[:2], 1, 1)
-    far_two = crossed(after[2:], 1, -1)
-    wm_a = (line, near, after, far_one, far_two)
-    wm_b = [swap(a) for a in wm_a[:3]]
-    wm_b += [swap(a) for a in wm_a[3:]]
+    far_one = crossed(near_one, 1, 1)
+    far_two = crossed(after_two, 1, -1)
+    wm_a = (line_one, line_two, near_one, near_two, after_one, after_two, far_one, far_two)
+    wm_b = [swap(a) for a in wm_a[:6]]
+    wm_b += [swap(a) for a in wm_a[6:]]
     outs = finish(
         place,
         whole,

time: 93.2 us -> 98.7 us (1.059)
  starting transfers between devices: 39 us -> 51.2 us
  waiting for transfers between devices: 26 us -> 21 us
  local copies, waits for them, and re-layouts: 1.72 us -> 0.06 us
    all_to_all x1, waiting for transfers between devices: 9.52 us -> 1.46 us  [body(): lax.all_to_all(partial.reshape(64, 16, 128), (*FAR, 'tp'), 0, 0, tiled=True)]
    ppermute x9 -> x12, starting transfers between devices: 11.8 us -> 18.5 us  [shift(): lax.ppermute(value, axis, [(i, (i + by) % size) for i in range(size)])]
    all_to_all x1, starting transfers between devices: 5.67 us -> 8.14 us  [body(): lax.all_to_all(partial.reshape(64, 16, 128), (*FAR, 'tp'), 0, 0, tiled=True)]
    ppermute x7 -> x9, starting transfers between devices: 8.22 us -> 10.1 us  [crossed(): return lax.ppermute(value, FS, pairs)]
    slice x2 -> x0, local copies, waits for them, and re-layouts: 1.67 us -> none  [the longest x1 1.65 us: body(): far_two = crossed(after[2:], 1, -1)]
    all_to_all x1, waiting for transfers between devices: 0.53 us -> 2.12 us  [body(): lax.all_to_all(packed.reshape(64, 16, 128), (*FAR, 'tp'), 0, 0, tiled=True)]
    all_to_all x1, starting transfers between devices: 4.73 us -> 5.88 us  [body(): lax.all_to_all(packed.reshape(64, 16, 128), (*FAR, 'tp'), 0, 0, tiled=True)]
    ppermute x7 -> x9, waiting for transfers between devices: 4.31 us -> 5.25 us  [crossed(): return lax.ppermute(value, FS, pairs)]
  transfers between devices with their start and end apart: 19 -> 24, of which waited for: 7 -> 9; matrix products, arithmetic and copies ran while one was open for 3% -> 1% of each run, Pallas kernels for 17% -> 16%
where the time goes in v1:
time: 98.7 us; the launch traced here: 98.3 us
  starting transfers between devices  51.2 us (52%)
  Pallas kernels  24.1 us (24%)
  waiting for transfers between devices  21 us (21%)
  between operations  1.1 us (1%)
    ppermute x12, starting transfers between devices, shift(): lax.ppermute(value, axis, [(i, (i + by) % size) for i in range(size)])  18.5 us
    pallas_call x1, Pallas kernels, grad_halves(): pl.pallas_call(grad_kernel, out_shape=(pltpu.HBM((768, 1024), jnp.bfloat1...  11.7 us
    all_to_all x1, waiting for transfers between devices, body(): p_a = lax.all_to_all(p_all, FAR, 0, 0, tiled=True)  10.3 us
    ppermute x9, starting transfers between devices, crossed(): return lax.ppermute(value, FS, pairs)  10.1 us
    all_to_all x1, starting transfers between devices, body(): p_a = lax.all_to_all(p_all, FAR, 0, 0, tiled=True)  8.59 us
    all_to_all x1, starting transfers between devices, body(): lax.all_to_all(partial.reshape(64, 16, 128), (*FAR, 'tp'), 0, 0, tiled=True)  8.14 us
    pallas_call x1, Pallas kernels, finish(): pl.pallas_call(finish_kernel, out_shape=(step,) * 3 + (rows, rows, turned...  6.51 us
    all_to_all x1, starting transfers between devices, body(): lax.all_to_all(packed.reshape(64, 16, 128), (*FAR, 'tp'), 0, 0, tiled=True)  5.88 us
  transfers between devices with their start and end apart: 24, of which 9 were waited for; matrix products, arithmetic and copies ran while one was open for 1% of the time, Pallas kernels for 16%

profile of v1, /device:TPU:1, one launch (start us, length us, event | category | flops | bytes accessed | tf_op | source)
XLA Modules:
  0.0 98.3 jit_solution(14618333962641721437)
XLA Ops:
  0.6 2.1 %spread.1 = bf16[16,64,768]{2,1,0:T(8,128)(2,1)} custom-call(bf16[64,256]{1,0:T(8,128)(2,1)} %refs_21_.1, bf16[64,256]{1,0:T(8,128)(2,1)} %refs_22_.1, bf16[64,256]{1,0:T(8,128)(2,1)} %refs_23_.1), custom_call_target="tpu_custom_call" | custom-call | tf_op jit(solution)/shard_map/spread/pallas_call | solution.py:56
  2.7 8.6 %all-to-all-start = ((bf16[16,64,768]{2,1,0:T(8,128)(2,1)}), bf16[16,64,768]{2,1,0:T(8,128)(2,1)S(1)}, u32[]{:S(2)}, u32[]{:S(2)}) async-start(bf16[16,64,768]{2,1,0:T(8,128)(2,1)} %spread.1), calls=%async_computation | async-start | bytes 3145728 | tf_op jit(solution)/shard_map/all_to_all | solution.py:510
  11.3 0.0 copy-start.8
  11.3 0.0 copy-start.7
  11.3 0.0 copy-start.6
  11.4 0.0 copy-start.9
  11.4 11.7 %grads.1 = (bf16[768,1024]{1,0:T(8,128)(2,1)}, bf16[768,1024]{1,0:T(8,128)(2,1)}) custom-call(s32[1]{0:T(128)} %bitcast.2.core_ref, bf16[2048,256]{1,0:T(8,128)(2,1)} %k_ref.1, bf16[2048,256]{1,0:T(8,128)(2,1)} %v_ref.1, bf16[2048,256]{1,0:T(8,128)(2,1)} %h_ref.1, bf16[2048,2048]{1,0:T(8,128)(2,1)} %x_ref.1, bf16[2048,2048]{1,0:T(8,128)(2,1)} %o_ref.1), custom_call_target="tpu_custom_call" | custom-call | tf_op jit(solution)/shard_map/grads/pallas_call | solution.py:158
  23.0 1.0 %collective-permute-start = (bf16[768,1024]{1,0:T(8,128)(2,1)}, bf16[768,1024]{1,0:T(8,128)(2,1)S(1)}, u32[]{:S(2)}, u32[]{:S(2)}) collective-permute-start(bf16[768,1024]{1,0:T(8,128)(2,1)} %get-tuple-element.25), channel_id=1, source_target_pairs={{0,4},{4,0},{1,5},{5,1},{2,6},{6,2},{3,7},{7,3},{8,12},{12,8},{9,1... | collective-permute-start | bytes 4718600 | tf_op jit(solution)/shard_map/ppermute | solution.py:29
  24.1 0.0 copy-done.7
  24.1 10.3 %all-to-all-done.refs_3_ = bf16[16,64,768]{2,1,0:T(8,128)(2,1)S(1)} async-done(((bf16[16,64,768]{2,1,0:T(8,128)(2,1)}), bf16[16,64,768]{2,1,0:T(8,128)(2,1)S(1)}, u32[]{:S(2)}, u32[]{:S(2)}) %all-to-all-start) | async-done | bytes 1572896 | tf_op jit(solution)/shard_map/all_to_all | solution.py:510
  34.4 2.4 %collective-permute-start.3 = (bf16[16,64,768]{2,1,0:T(8,128)(2,1)S(1)}, bf16[16,64,768]{2,1,0:T(8,128)(2,1)}, u32[]{:S(2)}, u32[]{:S(2)}) collective-permute-start(bf16[16,64,768]{2,1,0:T(8,128)(2,1)S(1)} %all-to-all-done.refs_3_), channel_id=1, source_target_pairs={{0,4},{4,0},{1,5},{5,1},{2,6},{6,2},{3,7},{7,3},{8,12},{12,8},{9,1... | collective-permute-start | bytes 4718600 | tf_op jit(solution)/shard_map/ppermute | solution.py:29
  36.8 0.0 collective-permute-done.recv_ref
  36.8 1.5 %pair_sum.1.parts_ref = bf16[3,256,1024]{2,1,0:T(8,128)(2,1)S(1)} custom-call(bf16[768,1024]{1,0:T(8,128)(2,1)} %get-tuple-element.24.keep_ref, bf16[768,1024]{1,0:T(8,128)(2,1)S(1)} %collective-permute-done.recv_ref), custom_call_target="tpu_custom_call" | custom-call | tf_op jit(solution)/shard_map/pair_sum/pallas_call | solution.py:196
  38.3 0.0 copy-start.10
  38.3 0.0 copy-start.11
  38.4 1.4 %project.1 = (f32[16,4,16,128]{3,2,1,0:T(8,128)S(1)}, bf16[16,4,16,128]{3,2,1,0:T(8,128)(2,1)}) custom-call(s32[1]{0:T(128)} %bitcast.2.core_ref, bf16[3,256,1024]{2,1,0:T(8,128)(2,1)S(1)} %pair_sum.1.parts_ref, bf16[1024,768]{1,0:T(8,128)(2,1)S(1)} %bitcast.15), custom_call_target="tpu_custom_call" | custom-call | tf_op jit(solution)/shard_map/project/pallas_call | solution.py:245
  39.8 0.1 collective-permute-start.1
  39.9 0.1 collective-permute-start.4
  40.0 2.7 %collective-permute-start.5 = (bf16[80,768]{1,0:T(8,128)(2,1)S(1)}, bf16[80,768]{1,0:T(8,128)(2,1)S(1)}, u32[]{:S(2)}, u32[]{:S(2)}) collective-permute-start(bf16[80,768]{1,0:T(8,128)(2,1)S(1)} %pad_maximum_fusion.own_ref), channel_id=1, source_target_pairs={{0,24},{4,100},{8,0},{12,108},{16,8},{20,116},{24,16},{28,124},{32... | collective-permute-start | bytes 368648 | tf_op jit(solution)/shard_map/ppermute | solution.py:42
  42.7 0.0 collective-permute-start.6
  42.7 2.6 %collective-permute-done.4.below_ref = bf16[80,768]{1,0:T(8,128)(2,1)S(1)} collective-permute-done((bf16[80,768]{1,0:T(8,128)(2,1)S(1)}, bf16[80,768]{1,0:T(8,128)(2,1)S(1)}, u32[]{:S(2)}, u32[]{:S(2)}) %collective-permute-start.4) | collective-permute-done | bytes 122912 | tf_op jit(solution)/shard_map/ppermute | solution.py:42
  45.2 0.6 collective-permute-done.5.above_ref
  45.8 2.1 %collective-permute-done.6.across_ref = bf16[80,768]{1,0:T(8,128)(2,1)S(1)} collective-permute-done((bf16[80,768]{1,0:T(8,128)(2,1)S(1)}, bf16[80,768]{1,0:T(8,128)(2,1)S(1)}, u32[]{:S(2)}, u32[]{:S(2)}) %collective-permute-start.6) | collective-permute-done | bytes 122912 | tf_op jit(solution)/shard_map/ppermute | solution.py:42
  47.9 0.0 copy-start
  48.0 0.1 collective-permute-start.10
  48.0 1.5 %collective-permute-start.8 = (bf16[2,80,768]{2,1,0:T(8,128)(2,1)S(1)}, bf16[2,80,768]{2,1,0:T(8,128)(2,1)S(1)}, u32[]{:S(2)}, u32[]{:S(2)}) collective-permute-start(bf16[2,80,768]{2,1,0:T(8,128)(2,1)S(1)} %get-tuple-element.29.refs_6_), channel_id=1, source_target_pairs={{0,32},{4,12},{8,40},{12,20},{16,48},{20,28},{24,56},{28,4},{32,64... | collective-permute-start | bytes 737288 | tf_op jit(solution)/shard_map/ppermute | solution.py:42
  49.5 0.0 collective-permute-start.7
  49.5 0.0 collective-permute-done.1
  49.5 0.8 add_convert_fusion
  50.3 8.1 %all-to-all-start.1 = ((bf16[64,16,128]{2,1,0:T(8,128)(2,1)}), bf16[64,16,128]{2,1,0:T(8,128)(2,1)S(1)}, u32[]{:S(2)}, u32[]{:S(2)}) async-start(bf16[64,16,128]{2,1,0:T(8,128)(2,1)} %bitcast.4), calls=%async_computation.1 | async-start | bytes 524288 | tf_op jit(solution)/shard_map/all_to_all | solution.py:526
  58.5 2.3 %collective-permute-start.9 = (bf16[2,80,768]{2,1,0:T(8,128)(2,1)S(1)}, bf16[2,80,768]{2,1,0:T(8,128)(2,1)}, u32[]{:S(2)}, u32[]{:S(2)}) collective-permute-start(bf16[2,80,768]{2,1,0:T(8,128)(2,1)S(1)} %get-tuple-element.28.refs_5_), channel_id=1, source_target_pairs={{0,96},{4,28},{8,104},{12,4},{16,112},{20,12},{24,120},{28,20},{32... | collective-permute-start | bytes 737288 | tf_op jit(solution)/shard_map/ppermute | solution.py:42
  60.7 0.0 collective-permute-done.7.refs_7_
  60.8 4.4 %collective-permute-start.13 = (bf16[2,80,768]{2,1,0:T(8,128)(2,1)S(1)}, bf16[2,80,768]{2,1,0:T(8,128)(2,1)S(1)}, u32[]{:S(2)}, u32[]{:S(2)}) collective-permute-start(bf16[2,80,768]{2,1,0:T(8,128)(2,1)S(1)} %get-tuple-element.28.refs_5_), channel_id=1, source_target_pairs={{0,4},{4,0},{1,5},{5,1},{2,6},{6,2},{3,7},{7,3},{8,12},{12,8},{9,1... | collective-permute-start | bytes 737288 | tf_op jit(solution)/shard_map/ppermute | solution.py:29
  65.1 0.0 collective-permute-done.10.refs_10_
  65.1 0.1 collective-permute-start.14
  65.2 0.0 collective-permute-done.8.refs_8_
  65.2 1.2 %collective-permute-start.11 = (bf16[2,80,768]{2,1,0:T(8,128)(2,1)S(1)}, bf16[2,80,768]{2,1,0:T(8,128)(2,1)}, u32[]{:S(2)}, u32[]{:S(2)}) collective-permute-start(bf16[2,80,768]{2,1,0:T(8,128)(2,1)S(1)} %collective-permute-done.7.refs_7_), channel_id=1, source_target_pairs={{0,32},{4,12},{8,40},{12,20},{16,48},{20,28},{24,56},{28,4},{32,64... | collective-permute-start | bytes 737288 | tf_op jit(solution)/shard_map/ppermute | solution.py:42
  66.5 1.5 %all-to-all-done.1 = bf16[64,16,128]{2,1,0:T(8,128)(2,1)S(1)} async-done(((bf16[64,16,128]{2,1,0:T(8,128)(2,1)}), bf16[64,16,128]{2,1,0:T(8,128)(2,1)S(1)}, u32[]{:S(2)}, u32[]{:S(2)}) %all-to-all-start.1) | async-done | bytes 262176 | tf_op jit(solution)/shard_map/all_to_all | solution.py:526
  67.9 0.9 reduce_pieces.1
  68.8 5.9 %all-to-all-start.2 = ((bf16[64,16,128]{2,1,0:T(8,128)(2,1)}), bf16[64,16,128]{2,1,0:T(8,128)(2,1)S(1)}, u32[]{:S(2)}, u32[]{:S(2)}) async-start(bf16[64,16,128]{2,1,0:T(8,128)(2,1)} %bitcast.6), calls=%async_computation.2 | async-start | bytes 524288 | tf_op jit(solution)/shard_map/all_to_all | solution.py:536
  74.7 0.0 collective-permute-done.9.refs_9_
  74.7 2.3 %collective-permute-start.12 = (bf16[2,80,768]{2,1,0:T(8,128)(2,1)S(1)}, bf16[2,80,768]{2,1,0:T(8,128)(2,1)}, u32[]{:S(2)}, u32[]{:S(2)}) collective-permute-start(bf16[2,80,768]{2,1,0:T(8,128)(2,1)S(1)} %collective-permute-done.10.refs_10_), channel_id=1, source_target_pairs={{0,96},{4,28},{8,104},{12,4},{16,112},{20,12},{24,120},{28,20},{32... | collective-permute-start | bytes 737288 | tf_op jit(solution)/shard_map/ppermute | solution.py:42
  77.0 0.0 collective-permute-done.13.refs_13_
  77.0 4.5 %collective-permute-start.15 = (bf16[2,80,768]{2,1,0:T(8,128)(2,1)S(1)}, bf16[2,80,768]{2,1,0:T(8,128)(2,1)}, u32[]{:S(2)}, u32[]{:S(2)}) collective-permute-start(bf16[2,80,768]{2,1,0:T(8,128)(2,1)S(1)} %collective-permute-done.7.refs_7_), channel_id=1, source_target_pairs={{0,4},{4,0},{1,5},{5,1},{2,6},{6,2},{3,7},{7,3},{8,12},{12,8},{9,1... | collective-permute-start | bytes 737288 | tf_op jit(solution)/shard_map/ppermute | solution.py:29
  81.5 0.0 collective-permute-done.14.refs_14_
  81.5 0.1 collective-permute-start.18
  81.6 0.0 collective-permute-done.11.refs_11_
  81.6 0.4 collective-permute-start.16
  82.0 0.0 collective-permute-done.12.refs_12_
  82.0 2.1 %all-to-all-done.2 = bf16[64,16,128]{2,1,0:T(8,128)(2,1)S(1)} async-done(((bf16[64,16,128]{2,1,0:T(8,128)(2,1)}), bf16[64,16,128]{2,1,0:T(8,128)(2,1)S(1)}, u32[]{:S(2)}, u32[]{:S(2)}) %all-to-all-start.2) | async-done | bytes 262176 | tf_op jit(solution)/shard_map/all_to_all | solution.py:536
  84.2 4.9 %collective-permute-start.2 = (bf16[16,4,16,128]{3,2,1,0:T(8,128)(2,1)S(1)}, bf16[16,4,16,128]{3,2,1,0:T(8,128)(2,1)S(1)}, u32[]{:S(2)}, u32[]{:S(2)}) collective-permute-start(bf16[16,4,16,128]{3,2,1,0:T(8,128)(2,1)S(1)} %bitcast.16), channel_id=1, source_target_pairs={{0,4},{4,0},{1,5},{5,1},{2,6},{6,2},{3,7},{7,3},{8,12},{12,8},{9,1... | collective-permute-start | bytes 786440 | tf_op jit(solution)/shard_map/ppermute | solution.py:29
  89.0 0.0 collective-permute-done.15.refs_15_
  89.1 0.1 collective-permute-start.17
  89.1 0.0 collective-permute-done.18.refs_18_
  89.1 0.4 collective-permute-start.19
  89.6 0.0 collective-permute-done.16.refs_16_
  89.6 0.1 collective-permute-start.20
  89.7 0.1 pad_add_fusion.refs_0_
  89.7 1.2 %collective-permute-done.17.refs_17_ = bf16[2,80,768]{2,1,0:T(8,128)(2,1)} collective-permute-done((bf16[2,80,768]{2,1,0:T(8,128)(2,1)}, bf16[2,80,768]{2,1,0:T(8,128)(2,1)}, u32[]{:S(2)}, u32[]{:S(2)}) %collective-permute-start.17) | collective-permute-done | bytes 245792 | tf_op jit(solution)/shard_map/ppermute | solution.py:29
  90.9 0.4 collective-permute-done.19.refs_19_
  91.3 0.4 collective-permute-done.20.refs_20_
  91.6 0.0 collective-permute-done.2.refs_2_
  91.6 0.0 collective-permute-done.3.refs_4_
  91.7 6.5 %finish.1 = (f32[64,256]{1,0:T(8,128)}, f32[64,256]{1,0:T(8,128)}, f32[64,256]{1,0:T(8,128)}, bf16[16,2,64,256]{3,2,1,0:T(8,128)(2,1)}, bf16[16,2,64,256]{3,2,1,...) custom-call(s32[3]{0:T(128)S(1)} %pad_add_fusion.refs_0_, ...), custom_call_target="tpu_custom_call" | custom-call | tf_op jit(solution)/shard_map/finish/pallas_call | solution.py:461
  (25 shorter events, 0.1 us)
Async XLA Ops:
  2.7 31.7 %all-to-all-start = ((bf16[16,64,768]{2,1,0:T(8,128)(2,1)}), bf16[16,64,768]{2,1,0:T(8,128)(2,1)S(1)}, u32[]{:S(2)}, u32[]{:S(2)}) async-start(bf16[16,64,768]{2,1,0:T(8,128)(2,1)} %spread.1), calls=%async_computation | async-start | bytes 3145728 | tf_op jit(solution)/shard_map/all_to_all | solution.py:510
  11.3 12.7 %copy-start.8 = (f32[2,8,256]{2,1,0:T(8,128)S(1)}, f32[2,8,256]{2,1,0:T(8,128)}, u32[]{:S(2)}) copy-start(f32[2,8,256]{2,1,0:T(8,128)} %refs_24_.1) | copy-start | bytes 49156
  11.3 12.7 %copy-start.7 = (f32[2,8,256]{2,1,0:T(8,128)S(1)}, f32[2,8,256]{2,1,0:T(8,128)}, u32[]{:S(2)}) copy-start(f32[2,8,256]{2,1,0:T(8,128)} %refs_25_.1) | copy-start | bytes 49156
  11.3 12.7 %copy-start.6 = (f32[2,8,256]{2,1,0:T(8,128)S(1)}, f32[2,8,256]{2,1,0:T(8,128)}, u32[]{:S(2)}) copy-start(f32[2,8,256]{2,1,0:T(8,128)} %refs_26_.1) | copy-start | bytes 49156
  11.4 25.4 %copy-start.9 = (f32[256,64]{0,1:T(8,128)S(1)}, f32[256,64]{0,1:T(8,128)}, u32[]{:S(2)}) copy-start(f32[256,64]{0,1:T(8,128)} %param.21) | copy-start | bytes 196612
  23.0 13.8 %collective-permute-start = (bf16[768,1024]{1,0:T(8,128)(2,1)}, bf16[768,1024]{1,0:T(8,128)(2,1)S(1)}, u32[]{:S(2)}, u32[]{:S(2)}) collective-permute-start(bf16[768,1024]{1,0:T(8,128)(2,1)} %get-tuple-element.25), channel_id=1, source_target_pairs={{0,4},{4,0},{1,5},{5,1},{2,6},{6,2},{3,7},{7,3},{8,12},{12,8},{9,1... | collective-permute-start | bytes 4718600 | tf_op jit(solution)/shard_map/ppermute | solution.py:29
  34.4 57.2 %collective-permute-start.3 = (bf16[16,64,768]{2,1,0:T(8,128)(2,1)S(1)}, bf16[16,64,768]{2,1,0:T(8,128)(2,1)}, u32[]{:S(2)}, u32[]{:S(2)}) collective-permute-start(bf16[16,64,768]{2,1,0:T(8,128)(2,1)S(1)} %all-to-all-done.refs_3_), channel_id=1, source_target_pairs={{0,4},{4,0},{1,5},{5,1},{2,6},{6,2},{3,7},{7,3},{8,12},{12,8},{9,1... | collective-permute-start | bytes 4718600 | tf_op jit(solution)/shard_map/ppermute | solution.py:29
  38.3 1.5 %copy-start.10 = (f32[64,256]{1,0:T(8,128)S(1)}, f32[64,256]{1,0:T(8,128)}, u32[]{:S(2)}) copy-start(f32[64,256]{1,0:T(8,128)} %param.19) | copy-start | bytes 196612
  38.3 1.5 %copy-start.11 = (f32[64,256]{1,0:T(8,128)S(1)}, f32[64,256]{1,0:T(8,128)}, u32[]{:S(2)}) copy-start(f32[64,256]{1,0:T(8,128)} %param.20) | copy-start | bytes 196612
  39.8 9.8 %collective-permute-start.1 = (bf16[16,4,16,128]{3,2,1,0:T(8,128)(2,1)}, bf16[16,4,16,128]{3,2,1,0:T(8,128)(2,1)S(1)}, u32[]{:S(2)}, u32[]{:S(2)}) collective-permute-start(bf16[16,4,16,128]{3,2,1,0:T(8,128)(2,1)} %get-tuple-element.27), channel_id=1, source_target_pairs={{0,4},{4,0},{1,5},{5,1},{2,6},{6,2},{3,7},{7,3},{8,12},{12,8},{9,1... | collective-permute-start | bytes 786440 | tf_op jit(solution)/shard_map/ppermute | solution.py:29
  39.9 5.3 %collective-permute-start.4 = (bf16[80,768]{1,0:T(8,128)(2,1)S(1)}, bf16[80,768]{1,0:T(8,128)(2,1)S(1)}, u32[]{:S(2)}, u32[]{:S(2)}) collective-permute-start(bf16[80,768]{1,0:T(8,128)(2,1)S(1)} %pad_maximum_fusion.own_ref), channel_id=1, source_target_pairs={{0,8},{4,36},{8,16},{12,44},{16,24},{20,52},{24,0},{28,60},{32,40}... | collective-permute-start | bytes 368648 | tf_op jit(solution)/shard_map/ppermute | solution.py:42
  40.0 5.8 %collective-permute-start.5 = (bf16[80,768]{1,0:T(8,128)(2,1)S(1)}, bf16[80,768]{1,0:T(8,128)(2,1)S(1)}, u32[]{:S(2)}, u32[]{:S(2)}) collective-permute-start(bf16[80,768]{1,0:T(8,128)(2,1)S(1)} %pad_maximum_fusion.own_ref), channel_id=1, source_target_pairs={{0,24},{4,100},{8,0},{12,108},{16,8},{20,116},{24,16},{28,124},{32... | collective-permute-start | bytes 368648 | tf_op jit(solution)/shard_map/ppermute | solution.py:42
  42.7 5.2 %collective-permute-start.6 = (bf16[80,768]{1,0:T(8,128)(2,1)S(1)}, bf16[80,768]{1,0:T(8,128)(2,1)S(1)}, u32[]{:S(2)}, u32[]{:S(2)}) collective-permute-start(bf16[80,768]{1,0:T(8,128)(2,1)S(1)} %pad_maximum_fusion.own_ref), channel_id=1, source_target_pairs={{0,16},{4,68},{8,24},{12,76},{16,0},{20,84},{24,8},{28,92},{32,48}... | collective-permute-start | bytes 368648 | tf_op jit(solution)/shard_map/ppermute | solution.py:42
  47.9 43.7 %copy-start = (bf16[2,80,768]{2,1,0:T(8,128)(2,1)}, bf16[2,80,768]{2,1,0:T(8,128)(2,1)S(1)}, u32[]{:S(2)}) copy-start(bf16[2,80,768]{2,1,0:T(8,128)(2,1)S(1)} %get-tuple-element.28.refs_5_) | copy-start | bytes 737284
  48.0 43.7 %copy-start.1 = (bf16[2,80,768]{2,1,0:T(8,128)(2,1)}, bf16[2,80,768]{2,1,0:T(8,128)(2,1)S(1)}, u32[]{:S(2)}) copy-start(bf16[2,80,768]{2,1,0:T(8,128)(2,1)S(1)} %get-tuple-element.29.refs_6_) | copy-start | bytes 737284
  48.0 17.2 %collective-permute-start.10 = (bf16[2,80,768]{2,1,0:T(8,128)(2,1)S(1)}, bf16[2,80,768]{2,1,0:T(8,128)(2,1)S(1)}, u32[]{:S(2)}, u32[]{:S(2)}) collective-permute-start(bf16[2,80,768]{2,1,0:T(8,128)(2,1)S(1)} %get-tuple-element.29.refs_6_), channel_id=1, source_target_pairs={{0,96},{4,28},{8,104},{12,4},{16,112},{20,12},{24,120},{28,20},{32... | collective-permute-start | bytes 737288 | tf_op jit(solution)/shard_map/ppermute | solution.py:42
  48.0 17.2 %collective-permute-start.8 = (bf16[2,80,768]{2,1,0:T(8,128)(2,1)S(1)}, bf16[2,80,768]{2,1,0:T(8,128)(2,1)S(1)}, u32[]{:S(2)}, u32[]{:S(2)}) collective-permute-start(bf16[2,80,768]{2,1,0:T(8,128)(2,1)S(1)} %get-tuple-element.29.refs_6_), channel_id=1, source_target_pairs={{0,32},{4,12},{8,40},{12,20},{16,48},{20,28},{24,56},{28,4},{32,64... | collective-permute-start | bytes 737288 | tf_op jit(solution)/shard_map/ppermute | solution.py:42
  49.5 11.3 %collective-permute-start.7 = (bf16[2,80,768]{2,1,0:T(8,128)(2,1)S(1)}, bf16[2,80,768]{2,1,0:T(8,128)(2,1)S(1)}, u32[]{:S(2)}, u32[]{:S(2)}) collective-permute-start(bf16[2,80,768]{2,1,0:T(8,128)(2,1)S(1)} %get-tuple-element.28.refs_5_), channel_id=1, source_target_pairs={{0,32},{4,12},{8,40},{12,20},{16,48},{20,28},{24,56},{28,4},{32,64... | collective-permute-start | bytes 737288 | tf_op jit(solution)/shard_map/ppermute | solution.py:42
  50.3 17.6 %all-to-all-start.1 = ((bf16[64,16,128]{2,1,0:T(8,128)(2,1)}), bf16[64,16,128]{2,1,0:T(8,128)(2,1)S(1)}, u32[]{:S(2)}, u32[]{:S(2)}) async-start(bf16[64,16,128]{2,1,0:T(8,128)(2,1)} %bitcast.4), calls=%async_computation.1 | async-start | bytes 524288 | tf_op jit(solution)/shard_map/all_to_all | solution.py:526
  58.5 16.2 %collective-permute-start.9 = (bf16[2,80,768]{2,1,0:T(8,128)(2,1)S(1)}, bf16[2,80,768]{2,1,0:T(8,128)(2,1)}, u32[]{:S(2)}, u32[]{:S(2)}) collective-permute-start(bf16[2,80,768]{2,1,0:T(8,128)(2,1)S(1)} %get-tuple-element.28.refs_5_), channel_id=1, source_target_pairs={{0,96},{4,28},{8,104},{12,4},{16,112},{20,12},{24,120},{28,20},{32... | collective-permute-start | bytes 737288 | tf_op jit(solution)/shard_map/ppermute | solution.py:42
  60.8 30.9 %copy-start.4 = (bf16[2,80,768]{2,1,0:T(8,128)(2,1)}, bf16[2,80,768]{2,1,0:T(8,128)(2,1)S(1)}, u32[]{:S(2)}) copy-start(bf16[2,80,768]{2,1,0:T(8,128)(2,1)S(1)} %collective-permute-done.7.refs_7_) | copy-start | bytes 737284
  60.8 16.2 %collective-permute-start.13 = (bf16[2,80,768]{2,1,0:T(8,128)(2,1)S(1)}, bf16[2,80,768]{2,1,0:T(8,128)(2,1)S(1)}, u32[]{:S(2)}, u32[]{:S(2)}) collective-permute-start(bf16[2,80,768]{2,1,0:T(8,128)(2,1)S(1)} %get-tuple-element.28.refs_5_), channel_id=1, source_target_pairs={{0,4},{4,0},{1,5},{5,1},{2,6},{6,2},{3,7},{7,3},{8,12},{12,8},{9,1... | collective-permute-start | bytes 737288 | tf_op jit(solution)/shard_map/ppermute | solution.py:29
  65.1 26.5 %copy-start.2 = (bf16[2,80,768]{2,1,0:T(8,128)(2,1)}, bf16[2,80,768]{2,1,0:T(8,128)(2,1)S(1)}, u32[]{:S(2)}) copy-start(bf16[2,80,768]{2,1,0:T(8,128)(2,1)S(1)} %collective-permute-done.10.refs_10_) | copy-start | bytes 737284
  65.1 16.4 %collective-permute-start.14 = (bf16[2,80,768]{2,1,0:T(8,128)(2,1)S(1)}, bf16[2,80,768]{2,1,0:T(8,128)(2,1)}, u32[]{:S(2)}, u32[]{:S(2)}) collective-permute-start(bf16[2,80,768]{2,1,0:T(8,128)(2,1)S(1)} %get-tuple-element.29.refs_6_), channel_id=1, source_target_pairs={{0,4},{4,0},{1,5},{5,1},{2,6},{6,2},{3,7},{7,3},{8,12},{12,8},{9,1... | collective-permute-start | bytes 737288 | tf_op jit(solution)/shard_map/ppermute | solution.py:29
  65.2 26.4 %copy-start.3 = (bf16[2,80,768]{2,1,0:T(8,128)(2,1)}, bf16[2,80,768]{2,1,0:T(8,128)(2,1)S(1)}, u32[]{:S(2)}) copy-start(bf16[2,80,768]{2,1,0:T(8,128)(2,1)S(1)} %collective-permute-done.8.refs_8_) | copy-start | bytes 737284
  65.2 16.4 %collective-permute-start.11 = (bf16[2,80,768]{2,1,0:T(8,128)(2,1)S(1)}, bf16[2,80,768]{2,1,0:T(8,128)(2,1)}, u32[]{:S(2)}, u32[]{:S(2)}) collective-permute-start(bf16[2,80,768]{2,1,0:T(8,128)(2,1)S(1)} %collective-permute-done.7.refs_7_), channel_id=1, source_target_pairs={{0,32},{4,12},{8,40},{12,20},{16,48},{20,28},{24,56},{28,4},{32,64... | collective-permute-start | bytes 737288 | tf_op jit(solution)/shard_map/ppermute | solution.py:42
  68.8 15.3 %all-to-all-start.2 = ((bf16[64,16,128]{2,1,0:T(8,128)(2,1)}), bf16[64,16,128]{2,1,0:T(8,128)(2,1)S(1)}, u32[]{:S(2)}, u32[]{:S(2)}) async-start(bf16[64,16,128]{2,1,0:T(8,128)(2,1)} %bitcast.6), calls=%async_computation.2 | async-start | bytes 524288 | tf_op jit(solution)/shard_map/all_to_all | solution.py:536
  74.7 7.3 %collective-permute-start.12 = (bf16[2,80,768]{2,1,0:T(8,128)(2,1)S(1)}, bf16[2,80,768]{2,1,0:T(8,128)(2,1)}, u32[]{:S(2)}, u32[]{:S(2)}) collective-permute-start(bf16[2,80,768]{2,1,0:T(8,128)(2,1)S(1)} %collective-permute-done.10.refs_10_), channel_id=1, source_target_pairs={{0,96},{4,28},{8,104},{12,4},{16,112},{20,12},{24,120},{28,20},{32... | collective-permute-start | bytes 737288 | tf_op jit(solution)/shard_map/ppermute | solution.py:42
  77.0 7.2 %copy-start.5 = (bf16[2,80,768]{2,1,0:T(8,128)(2,1)}, bf16[2,80,768]{2,1,0:T(8,128)(2,1)S(1)}, u32[]{:S(2)}) copy-start(bf16[2,80,768]{2,1,0:T(8,128)(2,1)S(1)} %collective-permute-done.13.refs_13_) | copy-start | bytes 737284
  77.0 12.0 %collective-permute-start.15 = (bf16[2,80,768]{2,1,0:T(8,128)(2,1)S(1)}, bf16[2,80,768]{2,1,0:T(8,128)(2,1)}, u32[]{:S(2)}, u32[]{:S(2)}) collective-permute-start(bf16[2,80,768]{2,1,0:T(8,128)(2,1)S(1)} %collective-permute-done.7.refs_7_), channel_id=1, source_target_pairs={{0,4},{4,0},{1,5},{5,1},{2,6},{6,2},{3,7},{7,3},{8,12},{12,8},{9,1... | collective-permute-start | bytes 737288 | tf_op jit(solution)/shard_map/ppermute | solution.py:29
  81.5 7.6 %collective-permute-start.18 = (bf16[2,80,768]{2,1,0:T(8,128)(2,1)S(1)}, bf16[2,80,768]{2,1,0:T(8,128)(2,1)}, u32[]{:S(2)}, u32[]{:S(2)}) collective-permute-start(bf16[2,80,768]{2,1,0:T(8,128)(2,1)S(1)} %collective-permute-done.10.refs_10_), channel_id=1, source_target_pairs={{0,4},{4,0},{1,5},{5,1},{2,6},{6,2},{3,7},{7,3},{8,12},{12,8},{9,1... | collective-permute-start | bytes 737288 | tf_op jit(solution)/shard_map/ppermute | solution.py:29
  81.6 8.0 %collective-permute-start.16 = (bf16[2,80,768]{2,1,0:T(8,128)(2,1)S(1)}, bf16[2,80,768]{2,1,0:T(8,128)(2,1)}, u32[]{:S(2)}, u32[]{:S(2)}) collective-permute-start(bf16[2,80,768]{2,1,0:T(8,128)(2,1)S(1)} %collective-permute-done.8.refs_8_), channel_id=1, source_target_pairs={{0,4},{4,0},{1,5},{5,1},{2,6},{6,2},{3,7},{7,3},{8,12},{12,8},{9,1... | collective-permute-start | bytes 737288 | tf_op jit(solution)/shard_map/ppermute | solution.py:29
  84.2 7.5 %collective-permute-start.2 = (bf16[16,4,16,128]{3,2,1,0:T(8,128)(2,1)S(1)}, bf16[16,4,16,128]{3,2,1,0:T(8,128)(2,1)S(1)}, u32[]{:S(2)}, u32[]{:S(2)}) collective-permute-start(bf16[16,4,16,128]{3,2,1,0:T(8,128)(2,1)S(1)} %bitcast.16), channel_id=1, source_target_pairs={{0,4},{4,0},{1,5},{5,1},{2,6},{6,2},{3,7},{7,3},{8,12},{12,8},{9,1... | collective-permute-start | bytes 786440 | tf_op jit(solution)/shard_map/ppermute | solution.py:29
  89.1 1.9 %collective-permute-start.17 = (bf16[2,80,768]{2,1,0:T(8,128)(2,1)}, bf16[2,80,768]{2,1,0:T(8,128)(2,1)}, u32[]{:S(2)}, u32[]{:S(2)}) collective-permute-start(bf16[2,80,768]{2,1,0:T(8,128)(2,1)} %collective-permute-done.9.refs_9_), channel_id=1, source_target_pairs={{0,4},{4,0},{1,5},{5,1},{2,6},{6,2},{3,7},{7,3},{8,12},{12,8},{9,1... | collective-permute-start | bytes 737288 | tf_op jit(solution)/shard_map/ppermute | solution.py:29
  89.1 2.1 %collective-permute-start.19 = (bf16[2,80,768]{2,1,0:T(8,128)(2,1)}, bf16[2,80,768]{2,1,0:T(8,128)(2,1)}, u32[]{:S(2)}, u32[]{:S(2)}) collective-permute-start(bf16[2,80,768]{2,1,0:T(8,128)(2,1)} %collective-permute-done.11.refs_11_), channel_id=1, source_target_pairs={{0,4},{4,0},{1,5},{5,1},{2,6},{6,2},{3,7},{7,3},{8,12},{12,8},{9,1... | collective-permute-start | bytes 737288 | tf_op jit(solution)/shard_map/ppermute | solution.py:29
  89.6 2.0 %collective-permute-start.20 = (bf16[2,80,768]{2,1,0:T(8,128)(2,1)}, bf16[2,80,768]{2,1,0:T(8,128)(2,1)}, u32[]{:S(2)}, u32[]{:S(2)}) collective-permute-start(bf16[2,80,768]{2,1,0:T(8,128)(2,1)} %collective-permute-done.12.refs_12_), channel_id=1, source_target_pairs={{0,4},{4,0},{1,5},{5,1},{2,6},{6,2},{3,7},{7,3},{8,12},{12,8},{9,1... | collective-permute-start | bytes 737288 | tf_op jit(solution)/shard_map/ppermute | solution.py:29
